TPU v7x, 256 devices: a whole 4x4x8 slice. The times are simulated.
256 devices in a mesh: sp: 32 (over z, x), fs: 4 (over y), tp: 2 (over core).
Axes of the slice: x: 4, y: 4, z: 8, core: 2. Of those that a mesh axis runs over, the one named last changes fastest.
Arguments:
- inputs: bfloat16 [4, 4096, 2048], P('fs', 'sp', 'tp'), may hold values from -6 to 6
- input_norm_scale: float32 [2048], replicated, may hold values from 0.1 to 1.9
- query_matrix: bfloat16 [2048, 512], P('sp', 'tp'), may hold values from -0.125 to 0.125
- key_matrix: bfloat16 [2048, 512], P('sp', 'tp'), may hold values from -0.125 to 0.125
- value_matrix: bfloat16 [2048, 512], P('sp', 'tp'), may hold values from -0.125 to 0.125
- decay_down_weight: bfloat16 [2048, 128], replicated, may hold values from -0.125 to 0.125
- decay_up_weight: bfloat16 [128, 512], P(None, 'tp'), may hold values from -1.1953125 to 1.1953125
- decay_bias_base: float32 [512], P('tp'), as said below
- decay_position_offset: float32 [4, 4096, 8], P('fs', 'sp', 'tp'), may hold values from -0.7 to 0.7
- extra_log_decay: float32 [4, 4096, 8], P('fs', 'sp', 'tp'), may hold values from -2.8 to 0, as said below
- correction_down_weight: bfloat16 [2048, 128], replicated, may hold values from -0.125 to 0.125
- correction_up_weight: bfloat16 [128, 512], P(None, 'tp'), may hold values from -1.1953125 to 1.1953125
- correction_rate_bias: float32 [512], P('tp'), as said below
- head_norm_scale: float32 [512], P('tp'), may hold values from 0.1 to 1.9
- starting_states: float32 [4, 2, 8, 64, 64], P('fs', None, 'tp'), may hold values from -384 to 384
- pointwise_value_weight: bfloat16 [2048, 1024], P('sp', 'tp'), may hold values from -0.125 to 0.125
- pointwise_gate_weight: bfloat16 [2048, 1024], P('sp', 'tp'), may hold values from -0.125 to 0.125
- depthwise_taps_weight: float32 [31, 1024], P(None, 'tp')
- channel_norm_scale: float32 [1024], P('tp'), may hold values from 0.1 to 1.9
- mixer_output_weight: bfloat16 [512, 2048], P('tp', 'sp'), may hold values from -0.15625 to 0.15625
- convolution_output_weight: bfloat16 [1024, 2048], P('tp', 'sp'), may hold values from -0.15625 to 0.15625
Outputs:
- mixed: bfloat16 [4, 4096, 2048], P('fs', ('sp', 'tp'))
Inputs may be any that keep to these rules, and one draw needn't show every extreme that they name: `decay_bias_base`: decay bases, one value for every channel. `correction_rate_bias`: correction-rate bases, one value for every channel. `extra_log_decay`: zero at all but a few positions of each sequence.
All inputs are finite; a program needn't handle non-finite values.
Results may differ from a plain program's by a relative error of at most 0.012.
Values may be sent and summed in bfloat16 or wider, within the bound.
No kernel may reach another device: no remote copies, remote signals or barrier semaphores. Data moves between devices by JAX's collectives and lax.ppermute only.
A program may use at most 64 MiB of HBM per device.

v0:
```python
import jax
import jax.numpy as jnp
from jax import lax
from jax.sharding import Mesh
from jax.sharding import PartitionSpec as P

ATTN_GROUP_SIZE = 64
SP = ("sp_0", "sp_1")
SP_TP = ("sp_0", "sp_1", "tp")


def neutral_like(x, identity):
    return jax.tree.map(
        lambda a, e: jnp.broadcast_to(jnp.asarray(e, a.dtype), a.shape), x, identity
    )


def carried_in(x, axes, combine, identity, reverse):
    before = start = neutral_like(x, identity)
    subtotal = x
    for axis in reversed(axes):
        length, here = (lax.axis_size(axis), lax.axis_index(axis))
        pieces = jax.tree.map(
            lambda part, kind: lax.all_gather(part.astype(kind), axis),
            subtotal,
            (jnp.bfloat16, jnp.bfloat16),
        )
        inside, subtotal = (start, start)
        for k in reversed(range(length)) if reverse else range(length):
            passed = k > here if reverse else k < here
            subtotal = combine(
                subtotal, jax.tree.map(lambda part, own: part[k].astype(own.dtype), pieces, x)
            )
            inside = jax.tree.map(lambda new, old: jnp.where(passed, new, old), subtotal, inside)
        before = combine(inside, before)
    return before


def padded_2(block, sides, width):
    for axis, dim in sides:
        count = lax.axis_size(axis)
        forward = [(i, i + 1) for i in range(count - 1)]
        backward = [(target, source) for source, target in forward]
        low = lax.ppermute(
            lax.slice_in_dim(block, block.shape[dim] - width, None, axis=dim), axis, forward
        )
        high = lax.ppermute(lax.slice_in_dim(block, 0, width, axis=dim), axis, backward)
        block = jnp.concatenate([low, block, high], axis=dim)
    return block


def total_of_pieces(x, axis):
    pieces = lax.all_gather(x, axis)
    return pieces.sum(axis=0)


def copy_for_each(x, axis):
    length = lax.axis_size(axis)
    return lax.all_to_all(jnp.broadcast_to(x[None], (length, *x.shape)), axis, 0, 0, tiled=True)


def laid_out(pieces, dim):
    shape = list(pieces.shape[1:])
    shape[dim] *= pieces.shape[0]
    return jnp.moveaxis(pieces, 0, dim).reshape(shape)


def gather_directly(x, axis, dim):
    pieces = copy_for_each(x, axis)
    return laid_out(pieces, dim)


def sent_together(arrays, axis, dim, along):
    both = jnp.concatenate(arrays, axis=along)
    whole, at, finished = (lax.all_gather(both, axis, axis=dim, tiled=True), 0, [])
    for a in arrays:
        finished.append(lax.slice_in_dim(whole, at, at + a.shape[along], axis=along))
        at += a.shape[along]
    return tuple(finished)


def whole_of(x, axes, dim):
    whole = x
    for number in range(len(axes) - 1, -1, -1):
        whole = lax.all_gather(whole, axes[number], axis=dim, tiled=True)
    return whole


def cut_along(x, dim, length):
    before, after = (x.shape[:dim], x.shape[dim + 1 :])
    return jnp.moveaxis(x.reshape(*before, length, -1, *after), dim, 0)


def sum_at_owner(x, axis, dim):
    length = lax.axis_size(axis)
    pieces = lax.all_to_all(cut_along(x, dim, length), axis, 0, 0, tiled=True)
    return jnp.sum(pieces.astype(jnp.float32), axis=0)


def split_heads(values):
    return values.reshape(values.shape[0], -1, ATTN_GROUP_SIZE)


def paired(values):
    return jnp.stack([values, jnp.flip(values, 0)], 1)


def local_step(stacked, inputs):
    fading_multiplier, unit_key, rated_key, keys, values, query = inputs
    projected = jnp.einsum("dhvk,dhk->dhv", stacked, unit_key)
    outer = values[..., None] * keys[:, :, None, :]
    added = jnp.concatenate([jnp.zeros_like(outer), outer], axis=2)
    stacked = (
        stacked * fading_multiplier[:, :, None, :]
        - projected[..., None] * rated_key[:, :, None, :]
        + added
    )
    return (stacked, jnp.einsum("dhvk,dhk->dhv", stacked, query))


def chain_pair(earlier, later):
    product = jnp.einsum("hij,hjk->hik", earlier[0], later[0])
    moved = jnp.einsum("hij,hjk->hik", earlier[1], later[0]) + later[1]
    return (product, moved)


def carry_in(initial_memory_matrix, prefix):
    return jnp.einsum("hij,hjk->hik", initial_memory_matrix, prefix[0]) + prefix[1]


def head_norm(summed, head_norm_scale):
    centered = summed - jnp.mean(summed, axis=-1, keepdims=True)
    scaled = centered * lax.rsqrt(jnp.mean(centered * centered, axis=-1, keepdims=True) + 0.00064)
    return (
        (scaled * head_norm_scale.reshape(-1, ATTN_GROUP_SIZE))
        .reshape(summed.shape[0], -1)
        .astype(jnp.bfloat16)
    )


def rounded(total):
    return lax.optimization_barrier(total.astype(jnp.bfloat16)).astype(jnp.float32)


def mixer_branch(
    normed,
    sums,
    decay_down_weight,
    decay_up_weight,
    decay_bias_base,
    decay_position_offset,
    extra_log_decay,
    correction_down_weight,
    correction_up_weight,
    correction_rate_bias,
    head_norm_scale,
    starting_states,
):
    query = rounded(sums[0])
    keys = rounded(sums[1])
    values = rounded(sums[2])
    low_decay = jnp.tanh(
        jnp.dot(normed, decay_down_weight, preferred_element_type=jnp.float32)
    ).astype(jnp.bfloat16)
    fading_raw_scores = (
        decay_bias_base
        + jnp.dot(low_decay, decay_up_weight, preferred_element_type=jnp.float32)
        + jnp.repeat(decay_position_offset[0], ATTN_GROUP_SIZE, axis=1)
    )
    fading_multiplier = jnp.exp(
        -jnp.exp(-jax.nn.softplus(-fading_raw_scores) - 0.5)
        + jnp.repeat(extra_log_decay[0], ATTN_GROUP_SIZE, axis=1)
    )
    low_rate = jnp.dot(normed, correction_down_weight, preferred_element_type=jnp.float32).astype(
        jnp.bfloat16
    )
    rate = jax.nn.sigmoid(
        correction_rate_bias
        + jnp.dot(low_rate, correction_up_weight, preferred_element_type=jnp.float32)
    )
    key_heads = split_heads(keys)
    unit_key = key_heads * lax.rsqrt(jnp.sum(key_heads * key_heads, axis=-1, keepdims=True) + 1e-06)
    rated_key = unit_key * split_heads(rate)
    steps = tuple(
        (
            paired(item)
            for item in (
                split_heads(fading_multiplier),
                unit_key,
                rated_key,
                key_heads,
                split_heads(values),
                split_heads(query),
            )
        )
    )
    heads_here = key_heads.shape[1]
    identity = jnp.broadcast_to(
        jnp.eye(ATTN_GROUP_SIZE, dtype=jnp.float32),
        (2, heads_here, ATTN_GROUP_SIZE, ATTN_GROUP_SIZE),
    )
    nothing = jnp.zeros((2, heads_here, ATTN_GROUP_SIZE, ATTN_GROUP_SIZE), jnp.float32)
    start = jnp.concatenate([identity, nothing], axis=2)
    ends, emitted = lax.scan(local_step, start, steps, unroll=8)
    transfer = ends[:, :, :ATTN_GROUP_SIZE]
    alone = ends[:, :, ATTN_GROUP_SIZE:]
    through = emitted[..., :ATTN_GROUP_SIZE]
    own_part = emitted[..., ATTN_GROUP_SIZE:]
    before = carried_in((transfer[0], alone[0]), SP, chain_pair, (identity[0], nothing[0]), False)
    after = carried_in((transfer[1], alone[1]), SP, chain_pair, (identity[1], nothing[1]), True)
    starts = jnp.stack(
        [carry_in(starting_states[0, 0], before), carry_in(starting_states[0, 1], after)], 0
    )
    outputs = jnp.einsum("dhvk,tdhk->tdhv", starts, through) + own_part
    summed = outputs[:, 0] + jnp.flip(outputs[:, 1], 0)
    return head_norm(summed, head_norm_scale)


def conv_branch(sums, depthwise_taps_weight, channel_norm_scale):
    glu = (sums[0] * jax.nn.sigmoid(sums[1])).astype(jnp.bfloat16)
    reach = depthwise_taps_weight.shape[0] // 2
    padded = padded_2(glu, ((SP, 0),), reach)
    conv = lax.conv_general_dilated(
        padded.astype(jnp.float32)[None],
        depthwise_taps_weight[:, None, :],
        (1,),
        "VALID",
        dimension_numbers=("NWC", "WIO", "NWC"),
        feature_group_count=depthwise_taps_weight.shape[1],
    )[0]
    first, second = (
        total_of_pieces(jnp.sum(conv, axis=-1), "tp"),
        total_of_pieces(jnp.sum(conv * conv, axis=-1), "tp"),
    )
    width = conv.shape[1] * lax.axis_size("tp")
    mean = first / width
    power = second / width - mean * mean
    return jax.nn.silu(
        (conv - mean[:, None]) * lax.rsqrt(power[:, None] + 1e-05) * channel_norm_scale
    ).astype(jnp.bfloat16)


def per_device(
    inputs,
    input_norm_scale,
    query_matrix,
    key_matrix,
    value_matrix,
    decay_down_weight,
    decay_up_weight,
    decay_bias_base,
    decay_position_offset,
    extra_log_decay,
    correction_down_weight,
    correction_up_weight,
    correction_rate_bias,
    head_norm_scale,
    starting_states,
    pointwise_value_weight,
    pointwise_gate_weight,
    depthwise_taps_weight,
    channel_norm_scale,
    mixer_output_weight,
    convolution_output_weight,
):
    symbol_vectors = gather_directly(inputs[0], "tp", 1)
    as_float = symbol_vectors.astype(jnp.float32)
    normed = (
        as_float
        * lax.rsqrt(jnp.mean(as_float * as_float, axis=-1, keepdims=True) + 1e-06)
        * input_norm_scale
    ).astype(jnp.bfloat16)
    mixer_args = (
        decay_down_weight,
        decay_up_weight,
        decay_bias_base,
        decay_position_offset,
        extra_log_decay,
        correction_down_weight,
        correction_up_weight,
        correction_rate_bias,
        head_norm_scale,
        starting_states,
    )
    collected = sent_together(
        (query_matrix, key_matrix, value_matrix, pointwise_value_weight, pointwise_gate_weight),
        SP,
        0,
        1,
    )
    sums = tuple(
        (jnp.dot(normed, weight, preferred_element_type=jnp.float32) for weight in collected)
    )
    mixer_out = mixer_branch(normed, sums[:3], *mixer_args)
    conv_out = conv_branch(sums[3:], depthwise_taps_weight, channel_norm_scale)
    joined = jnp.concatenate([mixer_out, conv_out], axis=1)
    weight_rows = jnp.concatenate([mixer_output_weight, convolution_output_weight], axis=0)
    columns = whole_of(weight_rows, SP, 1)
    block = lax.slice_in_dim(
        joined, 0, joined.shape[0] // lax.axis_size("tp") * lax.axis_size("tp"), axis=0
    )
    total = sum_at_owner(
        jnp.dot(block, columns, preferred_element_type=jnp.float32).astype(jnp.bfloat16), "tp", 0
    )
    return total.astype(jnp.bfloat16)[None]


def solution(mesh):
    finer = Mesh(
        mesh.devices.reshape(8, 4, mesh.shape["fs"], mesh.shape["tp"]), ("sp_0", "sp_1", "fs", "tp")
    )
    return jax.shard_map(
        per_device,
        mesh=finer,
        in_specs=(
            P("fs", SP, "tp"),
            P(),
            P(SP, "tp"),
            P(SP, "tp"),
            P(SP, "tp"),
            P(),
            P(None, "tp"),
            P("tp"),
            P("fs", SP, "tp"),
            P("fs", SP, "tp"),
            P(),
            P(None, "tp"),
            P("tp"),
            P("tp"),
            P("fs", None, "tp", None, None),
            P(SP, "tp"),
            P(SP, "tp"),
            P(None, "tp"),
            P("tp"),
            P("tp", SP),
            P("tp", SP),
        ),
        out_specs=P("fs", SP_TP, None),
        check_vma=False,
    )
```

profile of v0, /device:TPU:1, one launch (start us, length us, event | category | flops | bytes accessed | tf_op | source)
XLA Modules:
  0.0 516.0 jit_solution(5891452822749445654)
XLA Ops:
  13.4 6.7 %all-to-all-start = ((bf16[2,128,1024]{1,2,0:T(8,128)(2,1)}), bf16[2,128,1024]{1,2,0:T(8,128)(2,1)S(1)}, u32[]{:S(2)}, u32[]{:S(2)}) async-start(bf16[2,128,1024]{1,2,0:T(8,128)(2,1)} %broadcast_in_dim.77), calls=%async_computation | async-start | bytes 1048576 | tf_op jit(solution)/shard_map/all_to_all | solution.py:59
  20.9 10.4 %all_gather.78 = bf16[768,256]{0,1:T(8,128)(2,1)} all-gather(bf16[768,64]{0,1:T(8,128)(2,1)S(1)} %pad_maximum_fusion.6), channel_id=1, replica_groups=mesh['sp_0'=8,'sp_1'=4,'fs'=4,'tp'=2] {'sp_1'}, dimensions={1}, use_global_device_ids=true | all-gather | bytes 491520 | tf_op jit(solution)/shard_map/all_gather | solution.py:85
  32.7 1.3 fusion.86
  37.1 70.5 %all-gather.11.cloned.1.call-done = bf16[2048,1792]{1,0:T(8,128)(2,1)} async-done(((bf16[64,1792]{1,0:T(8,128)(2,1)}), bf16[2048,1792]{1,0:T(8,128)(2,1)}) %all-gather.11.cloned.1.call-update) | async-done | bytes 7340048 | tf_op jit(solution)/shard_map/all_gather | solution.py:75
  107.6 1.6 convolution_convert_fusion.1
  110.7 1.6 convolution_convert_fusion.2
  113.3 1.6 convolution_convert_fusion.3
  116.9 1.6 copy.129
  124.6 1.7 rev.25
  126.3 1.7 copy.123
  128.2 2.1 pad_maximum_fusion
  130.3 1.9 pad_maximum_fusion.2
  133.3 161.4 %while.12 = (s32[]{:T(128)}, f32[2,4,128,64]{3,2,1,0:T(8,128)S(1)}, f32[16,8,2,4,128]{4,1,0,3,2:T(8,128)S(1)}, f32[16,8,2,4,64]{4,1,0,3,2:T(8,128)}, bf16[16,8,2...) while((s32[]{:T(128)}, f32[2,4,128,64]{3,2,1,0:T(8,128)S(1)}, ...), condition=%wide.region_3.4_spmd, body=%wide.region_2.3_spmd.sunk | while | flops 6553609 | bytes 15270333 | solution.py:204
  133.5 1.6 constant_dynamic-slice_fusion.50
  135.1 1.6 constant_dynamic-slice_fusion.51
  144.0 1.3 constant_dynamic-slice_fusion.50
  145.3 1.4 constant_dynamic-slice_fusion.51
  154.0 1.3 constant_dynamic-slice_fusion.50
  155.3 1.7 constant_dynamic-slice_fusion.51
  164.2 1.3 constant_dynamic-slice_fusion.50
  165.5 1.6 constant_dynamic-slice_fusion.51
  174.3 1.3 constant_dynamic-slice_fusion.50
  175.6 1.6 constant_dynamic-slice_fusion.51
  184.5 1.3 constant_dynamic-slice_fusion.50
  185.8 1.3 constant_dynamic-slice_fusion.51
  194.3 1.3 constant_dynamic-slice_fusion.50
  195.6 1.3 constant_dynamic-slice_fusion.51
  204.2 1.3 constant_dynamic-slice_fusion.50
  205.5 1.5 constant_dynamic-slice_fusion.51
  214.3 1.2 constant_dynamic-slice_fusion.50
  215.5 1.6 constant_dynamic-slice_fusion.51
  225.6 1.6 constant_dynamic-slice_fusion.51
  234.4 1.3 constant_dynamic-slice_fusion.50
  235.8 1.3 constant_dynamic-slice_fusion.51
  244.3 1.3 constant_dynamic-slice_fusion.50
  245.6 1.6 constant_dynamic-slice_fusion.51
  254.4 1.3 constant_dynamic-slice_fusion.50
  255.7 1.5 constant_dynamic-slice_fusion.51
  264.5 1.3 constant_dynamic-slice_fusion.50
  265.8 1.6 constant_dynamic-slice_fusion.51
  274.6 1.3 constant_dynamic-slice_fusion.50
  275.9 1.6 constant_dynamic-slice_fusion.51
  284.8 1.3 constant_dynamic-slice_fusion.50
  286.1 1.6 constant_dynamic-slice_fusion.51
  294.7 9.4 %all_gather.62 = bf16[4,4,64,64]{3,2,1,0:T(8,128)(2,1)S(1)} all-gather(bf16[1,4,64,64]{3,2,1,0:T(8,128)(2,1)S(1)} %get-tuple-element.143), channel_id=1, replica_groups=mesh['sp_0'=8,'sp_1'=4,'fs'=4,'tp'=2] {'sp_1'}, dimensions={0}, use_global_device_ids=true | all-gather | bytes 163840 | tf_op jit(solution)/shard_map/all_gather | solution.py:24
  304.7 9.9 %all_gather.65 = bf16[4,4,64,64]{3,2,1,0:T(8,128)(2,1)S(1)} all-gather(bf16[1,4,64,64]{3,2,1,0:T(8,128)(2,1)S(1)} %get-tuple-element.146), channel_id=1, replica_groups=mesh['sp_0'=8,'sp_1'=4,'fs'=4,'tp'=2] {'sp_1'}, dimensions={0}, use_global_device_ids=true | all-gather | bytes 163840 | tf_op jit(solution)/shard_map/all_gather | solution.py:24
  315.2 19.4 %all-gather = bf16[32,64,64]{2,1,0:T(8,128)(2,1)S(1)} all-gather(bf16[4,64,64]{2,1,0:T(8,128)(2,1)S(1)} %fusion.243), channel_id=2, replica_groups=mesh['sp_0'=8,'sp_1'=4,'fs'=4,'tp'=2] {'sp_0'}, dimensions={0}, use_global_device_ids=true | all-gather | bytes 294912 | tf_op jit(solution)/shard_map/all_gather | solution.py:24
  336.3 19.3 %all-gather.1 = bf16[32,64,64]{2,1,0:T(8,128)(2,1)S(1)} all-gather(bf16[4,64,64]{2,1,0:T(8,128)(2,1)S(1)} %convolution_add_fusion.19), channel_id=3, replica_groups=mesh['sp_0'=8,'sp_1'=4,'fs'=4,'tp'=2] {'sp_0'}, dimensions={0}, use_global_device_ids=true | all-gather | bytes 294912 | tf_op jit(solution)/shard_map/all_gather | solution.py:24
  355.6 2.1 fusion.64
  357.7 2.1 fusion.68
  360.4 1.9 collective-permute-start
  362.4 1.3 collective-permute-start.1
  363.7 11.4 %all_gather.68 = bf16[4,4,64,64]{3,2,1,0:T(8,128)(2,1)S(1)} all-gather(bf16[1,4,64,64]{3,2,1,0:T(8,128)(2,1)S(1)} %get-tuple-element.145), channel_id=1, replica_groups=mesh['sp_0'=8,'sp_1'=4,'fs'=4,'tp'=2] {'sp_1'}, dimensions={0}, use_global_device_ids=true | all-gather | bytes 163840 | tf_op jit(solution)/shard_map/all_gather | solution.py:24
  376.8 9.4 %all_gather.71 = bf16[4,4,64,64]{3,2,1,0:T(8,128)(2,1)S(1)} all-gather(bf16[1,4,64,64]{3,2,1,0:T(8,128)(2,1)S(1)} %get-tuple-element.144), channel_id=1, replica_groups=mesh['sp_0'=8,'sp_1'=4,'fs'=4,'tp'=2] {'sp_1'}, dimensions={0}, use_global_device_ids=true | all-gather | bytes 163840 | tf_op jit(solution)/shard_map/all_gather | solution.py:24
  387.4 22.3 %all-gather.2 = bf16[32,64,64]{2,1,0:T(8,128)(2,1)S(1)} all-gather(bf16[4,64,64]{2,1,0:T(8,128)(2,1)S(1)} %fusion.246), channel_id=4, replica_groups=mesh['sp_0'=8,'sp_1'=4,'fs'=4,'tp'=2] {'sp_0'}, dimensions={0}, use_global_device_ids=true | all-gather | bytes 294912 | tf_op jit(solution)/shard_map/all_gather | solution.py:24
  416.3 21.2 %all-gather.3 = bf16[32,64,64]{2,1,0:T(8,128)(2,1)} all-gather(bf16[4,64,64]{2,1,0:T(8,128)(2,1)S(1)} %convolution_add_fusion.7), channel_id=5, replica_groups=mesh['sp_0'=8,'sp_1'=4,'fs'=4,'tp'=2] {'sp_0'}, dimensions={0}, use_global_device_ids=true | all-gather | bytes 294912 | tf_op jit(solution)/shard_map/all_gather | solution.py:24
  438.1 1.2 fusion.82
  439.4 1.3 fusion.75
  452.1 1.3 fusion.81
  456.4 4.4 fusion.310
  460.8 38.2 %all-gather.6 = f32[2,1,128]{2,1,0:T(1,128)S(1)} all-gather(f32[1,1,128]{2,1,0:T(1,128)S(1)} %bitcast.747), channel_id=6, replica_groups=mesh['sp_0'=8,'sp_1'=4,'fs'=4,'tp'=2] {'tp'}, dimensions={0}, use_global_device_ids=true | all-gather | bytes 1536 | tf_op jit(solution)/shard_map/all_gather | solution.py:53
  499.1 1.8 all-gather.7
  501.1 3.0 convolution_convert_fusion
  504.2 4.1 all_to_all.10
  (794 shorter events, 167.4 us)
Async XLA Ops:
  6.5 26.2 %copy-start = (bf16[2048,128]{1,0:T(8,128)(2,1)S(1)}, bf16[2048,128]{1,0:T(8,128)(2,1)}, u32[]{:S(2)}) copy-start(bf16[2048,128]{1,0:T(8,128)(2,1)} %param.33) | copy-start | bytes 1572868
  6.5 27.8 %copy-start.30 = (f32[1,128,4]{1,2,0:T(4,128)S(1)}, f32[1,128,4]{1,2,0:T(4,128)}, u32[]{:S(2)}) copy-start(f32[1,128,4]{1,2,0:T(4,128)} %param.31) | copy-start | bytes 6148
  6.5 27.9 %copy-start.31 = (f32[1,128,4]{1,2,0:T(4,128)S(1)}, f32[1,128,4]{1,2,0:T(4,128)}, u32[]{:S(2)}) copy-start(f32[1,128,4]{1,2,0:T(4,128)} %param.32) | copy-start | bytes 6148
  6.5 28.0 %copy-start.33 = (f32[256]{0:T(256)S(1)}, f32[256]{0:T(256)}, u32[]{:S(2)}) copy-start(f32[256]{0:T(256)} %param.30) | copy-start | bytes 3076
  6.5 28.0 %copy-start.27 = (bf16[128,256]{1,0:T(8,128)(2,1)S(1)}, bf16[128,256]{1,0:T(8,128)(2,1)}, u32[]{:S(2)}) copy-start(bf16[128,256]{1,0:T(8,128)(2,1)} %param.29) | copy-start | bytes 196612
  6.5 28.0 %copy-start.5 = (bf16[2048,128]{1,0:T(8,128)(2,1)S(1)}, bf16[2048,128]{1,0:T(8,128)(2,1)}, u32[]{:S(2)}) copy-start(bf16[2048,128]{1,0:T(8,128)(2,1)} %param.28) | copy-start | bytes 1572868
  6.6 28.9 %copy-start.34 = (f32[256]{0:T(256)S(1)}, f32[256]{0:T(256)}, u32[]{:S(2)}) copy-start(f32[256]{0:T(256)} %param.36) | copy-start | bytes 3076
  6.6 101.1 %all-gather.11.cloned.1.call-start = ((), (), s32[]{:S(2)}) async-start(), calls=%async_computation.2 | async-start | bytes 7569408 | tf_op jit(solution)/shard_map/all_gather | solution.py:75
  10.7 0.7 copy-start.6
  13.4 18.0 %all-to-all-start = ((bf16[2,128,1024]{1,2,0:T(8,128)(2,1)}), bf16[2,128,1024]{1,2,0:T(8,128)(2,1)S(1)}, u32[]{:S(2)}, u32[]{:S(2)}) async-start(bf16[2,128,1024]{1,2,0:T(8,128)(2,1)} %broadcast_in_dim.77), calls=%async_computation | async-start | bytes 1048576 | tf_op jit(solution)/shard_map/all_to_all | solution.py:59
  20.0 481.1 %all-gather.13.cloned.1.call-start = ((), (), s32[]{:S(2)}) async-start(), calls=%async_computation.3 | async-start | bytes 3538944 | tf_op jit(solution)/shard_map/all_gather | solution.py:85
  359.8 77.9 %copy-start.1 = (bf16[128,512]{1,0:T(8,128)(2,1)}, bf16[128,512]{1,0:T(8,128)(2,1)S(1)}, u32[]{:S(2)}) copy-start(bf16[128,512]{1,0:T(8,128)(2,1)S(1)} %fusion.68) | copy-start | bytes 393220
  360.4 95.9 %collective-permute-start = (bf16[15,512]{1,0:T(8,128)(2,1)}, bf16[15,512]{1,0:T(8,128)(2,1)S(1)}, u32[]{:S(2)}, u32[]{:S(2)}) collective-permute-start(bf16[15,512]{1,0:T(8,128)(2,1)} %get-tuple-element.148), channel_id=1, source_target_pairs={{0,8},{8,16},{16,24},{24,32},{32,40},{40,48},{48,56},{56,64},{64,7... | collective-permute-start | bytes 46088 | tf_op jit(solution)/shard_map/ppermute | solution.py:44
  362.4 94.0 %collective-permute-start.1 = (bf16[15,512]{1,0:T(8,128)(2,1)S(1)}, bf16[15,512]{1,0:T(8,128)(2,1)S(1)}, u32[]{:S(2)}, u32[]{:S(2)}) collective-permute-start(bf16[15,512]{1,0:T(8,128)(2,1)S(1)} %get-tuple-element.149), channel_id=1, source_target_pairs={{8,0},{16,8},{24,16},{32,24},{40,32},{48,40},{56,48},{64,56},{72,6... | collective-permute-start | bytes 46088 | tf_op jit(solution)/shard_map/ppermute | solution.py:47
  375.3 0.6 copy-start.19
  376.0 0.6 copy-start.10
  376.2 0.6 copy-start.11
  376.8 32.9 %copy-start.12 = (bf16[4,64,64]{2,1,0:T(8,128)(2,1)}, bf16[4,64,64]{2,1,0:T(8,128)(2,1)S(1)}, u32[]{:S(2)}) copy-start(bf16[4,64,64]{2,1,0:T(8,128)(2,1)S(1)} %fusion.246) | copy-start | bytes 98308
  386.3 0.6 copy-start.21
  387.1 50.5 %copy-start.3 = (bf16[4,64,64]{2,1,0:T(8,128)(2,1)}, bf16[4,64,64]{2,1,0:T(8,128)(2,1)S(1)}, u32[]{:S(2)}) copy-start(bf16[4,64,64]{2,1,0:T(8,128)(2,1)S(1)} %convolution_add_fusion.9) | copy-start | bytes 98308
  387.2 50.4 %copy-start.4 = (bf16[4,64,64]{2,1,0:T(8,128)(2,1)}, bf16[4,64,64]{2,1,0:T(8,128)(2,1)S(1)}, u32[]{:S(2)}) copy-start(bf16[4,64,64]{2,1,0:T(8,128)(2,1)S(1)} %convolution_add_fusion.8) | copy-start | bytes 98308
  409.9 0.6 copy-start.18
  410.6 27.0 %copy-start.7 = (bf16[4,64,64]{2,1,0:T(8,128)(2,1)}, bf16[4,64,64]{2,1,0:T(8,128)(2,1)S(1)}, u32[]{:S(2)}) copy-start(bf16[4,64,64]{2,1,0:T(8,128)(2,1)S(1)} %fusion.266) | copy-start | bytes 98308
  410.8 26.9 %copy-start.8 = (bf16[4,64,64]{2,1,0:T(8,128)(2,1)}, bf16[4,64,64]{2,1,0:T(8,128)(2,1)S(1)}, u32[]{:S(2)}) copy-start(bf16[4,64,64]{2,1,0:T(8,128)(2,1)S(1)} %fusion.263) | copy-start | bytes 98308
  410.9 26.8 %copy-start.9 = (bf16[4,64,64]{2,1,0:T(8,128)(2,1)}, bf16[4,64,64]{2,1,0:T(8,128)(2,1)S(1)}, u32[]{:S(2)}) copy-start(bf16[4,64,64]{2,1,0:T(8,128)(2,1)S(1)} %fusion.260) | copy-start | bytes 98308
  411.9 0.6 copy-start.20
  412.6 24.9 %copy-start.13 = (bf16[4,64,64]{2,1,0:T(8,128)(2,1)}, bf16[4,64,64]{2,1,0:T(8,128)(2,1)S(1)}, u32[]{:S(2)}) copy-start(bf16[4,64,64]{2,1,0:T(8,128)(2,1)S(1)} %fusion.290) | copy-start | bytes 98308
  412.8 24.8 %copy-start.14 = (bf16[4,64,64]{2,1,0:T(8,128)(2,1)}, bf16[4,64,64]{2,1,0:T(8,128)(2,1)S(1)}, u32[]{:S(2)}) copy-start(bf16[4,64,64]{2,1,0:T(8,128)(2,1)S(1)} %fusion.287) | copy-start | bytes 98308
  412.9 24.6 %copy-start.15 = (bf16[4,64,64]{2,1,0:T(8,128)(2,1)}, bf16[4,64,64]{2,1,0:T(8,128)(2,1)S(1)}, u32[]{:S(2)}) copy-start(bf16[4,64,64]{2,1,0:T(8,128)(2,1)S(1)} %fusion.284) | copy-start | bytes 98308
  413.1 24.5 %copy-start.16 = (bf16[4,64,64]{2,1,0:T(8,128)(2,1)}, bf16[4,64,64]{2,1,0:T(8,128)(2,1)S(1)}, u32[]{:S(2)}) copy-start(bf16[4,64,64]{2,1,0:T(8,128)(2,1)S(1)} %fusion.281) | copy-start | bytes 98308
  413.2 24.4 %copy-start.17 = (bf16[4,64,64]{2,1,0:T(8,128)(2,1)}, bf16[4,64,64]{2,1,0:T(8,128)(2,1)S(1)}, u32[]{:S(2)}) copy-start(bf16[4,64,64]{2,1,0:T(8,128)(2,1)S(1)} %fusion.278) | copy-start | bytes 98308
  414.2 0.6 copy-start.28
  414.9 22.7 %copy-start.22 = (bf16[4,64,64]{2,1,0:T(8,128)(2,1)}, bf16[4,64,64]{2,1,0:T(8,128)(2,1)S(1)}, u32[]{:S(2)}) copy-start(bf16[4,64,64]{2,1,0:T(8,128)(2,1)S(1)} %convolution_add_fusion.18) | copy-start | bytes 98308
  415.1 22.5 %copy-start.23 = (bf16[4,64,64]{2,1,0:T(8,128)(2,1)}, bf16[4,64,64]{2,1,0:T(8,128)(2,1)S(1)}, u32[]{:S(2)}) copy-start(bf16[4,64,64]{2,1,0:T(8,128)(2,1)S(1)} %convolution_add_fusion.17) | copy-start | bytes 98308
  415.2 22.4 %copy-start.24 = (bf16[4,64,64]{2,1,0:T(8,128)(2,1)}, bf16[4,64,64]{2,1,0:T(8,128)(2,1)S(1)}, u32[]{:S(2)}) copy-start(bf16[4,64,64]{2,1,0:T(8,128)(2,1)S(1)} %convolution_add_fusion.16) | copy-start | bytes 98308
  415.4 22.2 %copy-start.25 = (bf16[4,64,64]{2,1,0:T(8,128)(2,1)}, bf16[4,64,64]{2,1,0:T(8,128)(2,1)S(1)}, u32[]{:S(2)}) copy-start(bf16[4,64,64]{2,1,0:T(8,128)(2,1)S(1)} %convolution_add_fusion.15) | copy-start | bytes 98308
  415.6 22.1 %copy-start.26 = (bf16[4,64,64]{2,1,0:T(8,128)(2,1)}, bf16[4,64,64]{2,1,0:T(8,128)(2,1)S(1)}, u32[]{:S(2)}) copy-start(bf16[4,64,64]{2,1,0:T(8,128)(2,1)S(1)} %convolution_add_fusion.14) | copy-start | bytes 98308
  438.1 18.3 %copy-start.2 = (bf16[128,512]{1,0:T(8,128)(2,1)S(1)}, bf16[128,512]{1,0:T(8,128)(2,1)}, u32[]{:S(2)}) copy-start(bf16[128,512]{1,0:T(8,128)(2,1)} %copy-done.1) | copy-start | bytes 393220
  440.7 15.4 %copy-start.29 = (f32[4,64]{1,0:T(4,128)S(1)}, f32[4,64]{1,0:T(4,128)}, u32[]{:S(2)}) copy-start(f32[4,64]{1,0:T(4,128)} %mul.467) | copy-start | bytes 3076
  440.7 15.7 %copy-start.35 = (f32[31,512]{1,0:T(8,128)S(1)}, f32[31,512]{1,0:T(8,128)}, u32[]{:S(2)}) copy-start(f32[31,512]{1,0:T(8,128)} %param.40) | copy-start | bytes 190468
  442.8 58.1 %copy-start.32 = (f32[512]{0:T(512)S(1)}, f32[512]{0:T(512)}, u32[]{:S(2)}) copy-start(f32[512]{0:T(512)} %param.41) | copy-start | bytes 6148
Sparse Core Ops, SparseCore 0:
  11.5 96.0 all-gather.10
  109.4 42.1 all-gather.12
where the time goes:
time: 522 us; the launch traced here: 516 us
  blocking collectives  177 us (34%)
  matrix products  117 us (22%)
  local copies, waits for them, and re-layouts  76.1 us (15%)
  waiting for transfers between devices  70.6 us (14%)
  other arithmetic  48.9 us (9%)
  between operations  14.4 us (3%)
  starting transfers between devices  9.95 us (2%)
    all_gather x8, blocking collectives, carried_in(): lax.all_gather(part.astype(kind), axis)  122 us
    all_gather x1, waiting for transfers between devices, sent_together(): lax.all_gather(both, axis, axis=dim, tiled=True)  70.5 us
    slice x32, local copies, waits for them, and re-layouts, mixer_branch(): ends, emitted = lax.scan(local_step, start, steps, unroll=8)  45.5 us
    all_gather x2, blocking collectives, total_of_pieces(): pieces = lax.all_gather(x, axis)  40 us
    dot_general x128, matrix products, local_step(): projected = jnp.einsum('dhvk,dhk->dhv', stacked, unit_key)  36.5 us
    dot_general x128, matrix products, local_step(): return (stacked, jnp.einsum('dhvk,dhk->dhv', stacked, query))  36 us
    add x64, other arithmetic, local_step(): stacked * fading_multiplier[:, :, None, :]  22.6 us
    mul x128, other arithmetic, local_step(): outer = values[..., None] * keys[:, :, None, :]  16.7 us
  transfers between devices with their start and end apart: 5, of which 1 were waited for; matrix products, arithmetic and copies ran while one was open for 45% of the time, Pallas kernels for 0%

commit v1 on v0

v1 whole, which is shorter than its diff:
```python
import jax
import jax.numpy as jnp
from jax import lax
from jax.experimental import pallas as pl
from jax.experimental.pallas import tpu as pltpu
from jax.sharding import Mesh
from jax.sharding import PartitionSpec as P

BF = jnp.bfloat16
F32 = jnp.float32
CH = 64
ROWS = 512
GRP = 256
VM = pl.BlockSpec(memory_space=pltpu.VMEM)
SM = pl.BlockSpec(memory_space=pltpu.SMEM)


def call(body, outs, n_smem, n_vmem, scratch=(), flops=0, name=None):
    return pl.pallas_call(
        body,
        out_shape=[jax.ShapeDtypeStruct(s, d) for s, d in outs],
        in_specs=[SM] * n_smem + [VM] * n_vmem,
        out_specs=[VM] * len(outs),
        scratch_shapes=list(scratch),
        cost_estimate=pl.CostEstimate(flops=flops, bytes_accessed=0, transcendentals=0),
        name=name,
    )


def dot(a, b):
    return jnp.dot(a, b, preferred_element_type=F32)


def dot_nt(a, b):
    return lax.dot_general(a, b, (((1,), (1,)), ((), ())), preferred_element_type=F32)


def dot_tn(a, b, precision=None):
    return lax.dot_general(
        a, b, (((0,), (0,)), ((), ())), preferred_element_type=F32, precision=precision
    )


def low_lanes(shape):
    return lax.broadcasted_iota(jnp.int32, shape, len(shape) - 1) < CH


def half_roll(v):
    return pltpu.roll(v, CH, v.ndim - 1)


SHIFTS = (0, 1, -1, 2)


def prepare_body(
    idx, a0, a1, a2, a3, p0, p1, p2, p3, m0, m1, m2, m3, scale, ddw, cdw, dup, cup, db, cb,
    normed, pu, pr, pq, rate, pos, spike,
):
    x, c = idx[1], idx[3]
    mine = pl.multiple_of(c * 1024, 1024)
    other = pl.multiple_of((1 - c) * 1024, 1024)
    row8 = lax.broadcasted_iota(jnp.int32, (8, 128), 0)
    pick_pos = (row8 == x).astype(F32)
    pick_spike = (row8 == x + 4).astype(F32)
    for shift, a, p, m in zip(SHIFTS, (a0, a1, a2, a3), (p0, p1, p2, p3), (m0, m1, m2, m3)):
        row0 = pl.multiple_of(lax.rem(x - shift + 4, 4) * 128, 128)

        def rows(i, carry, a=a, p=p, row0=row0):
            r = pl.ds(pl.multiple_of(i * 16, 16), 16)
            to = pl.ds(pl.multiple_of(row0 + i * 16, 16), 16)
            own = a[r, :].astype(F32)
            far = p[r, :].astype(F32)
            power = jnp.sum(own * own, axis=1, keepdims=True) + jnp.sum(
                far * far, axis=1, keepdims=True
            )
            inv = lax.rsqrt(power * (1.0 / 2048) + 1e-6)
            normed[to, pl.ds(mine, 1024)] = (own * inv * scale[pl.ds(c, 1), :]).astype(BF)
            normed[to, pl.ds(other, 1024)] = (far * inv * scale[pl.ds(1 - c, 1), :]).astype(BF)
            return carry

        lax.fori_loop(0, 8, rows, 0)
        block = m[...]
        pos[pl.ds(row0, 128), :] = dot_tn(block, pick_pos, lax.Precision.HIGHEST)
        spike[pl.ds(row0, 128), :] = dot_tn(block, pick_spike, lax.Precision.HIGHEST)
    low = dot(normed[...], jnp.concatenate([ddw[...], cdw[...]], axis=1))
    low_decay = jnp.tanh(low[:, :128]).astype(BF)
    low_rate = low[:, 128:].astype(BF)
    pre = db[...] + dot(low_decay, dup[...]) + pos[...]
    logd = spike[...] - jax.nn.sigmoid(pre) * 0.6065306597126334
    rate[...] = jax.nn.sigmoid(cb[...] + dot(low_rate, cup[...]))
    lo = low_lanes((ROWS, 128))
    head = logd.astype(BF)
    tail = (logd - head.astype(F32)).astype(BF)
    parts = jnp.where(lo, head, tail)
    t = lax.broadcasted_iota(jnp.int32, (GRP, GRP), 0)
    s = lax.broadcasted_iota(jnp.int32, (GRP, GRP), 1)
    same = t // CH == s // CH
    mid = (s // CH) * CH + CH // 2
    sign = jnp.where(same & (s >= mid) & (s < t), 1.0, 0.0) - jnp.where(
        same & (s < mid) & (s >= t), 1.0, 0.0
    )
    sign = sign.astype(BF)
    both = jnp.concatenate([dot(sign, parts[:GRP]), dot(sign, parts[GRP:])], axis=0)
    before = both + half_roll(both)
    upto = before + logd
    pu[...] = jnp.exp(jnp.where(lo, before, -upto))
    pr[...] = jnp.exp(jnp.where(lo, -upto, before))
    pq[...] = jnp.exp(jnp.where(lo, upto, -before))


def prepare(*args):
    full = ((ROWS, 128), F32)
    return call(
        prepare_body,
        [((ROWS, 2048), BF), full, full, full, full],
        1,
        19,
        [pltpu.VMEM((ROWS, 128), F32), pltpu.VMEM((ROWS, 128), F32)],
        flops=2 * ROWS * 2048 * 256,
        name="prepare",
    )(*args)


def chunk_gain(pq, j):
    top = pq[pl.ds(j * CH, 1), :]
    bottom = pq[pl.ds(j * CH + CH - 1, 1), :]
    return jnp.where(low_lanes((1, 128)), bottom, top)


def maps_body(idx, normed, wkv, pu, pr, pq, rate, send, resp, rs_out, ks_out, kv_out, pre_out, xs, ta):
    kv = dot(normed[...], wkv[...]).astype(BF)
    kv_out[...] = kv
    kvf = kv.astype(F32)
    lo = low_lanes((ROWS, 128))
    turned = half_roll(kvf)
    kk = jnp.where(lo, kvf, turned)
    norm = lax.rsqrt(jnp.sum(kk * kk, axis=1, keepdims=True) * 0.5 + 1e-6)
    unit = kk * norm
    us = unit * pu[...]
    rsf = unit * rate[...] * pr[...]
    ksf = kk * pr[...]
    rs = rsf.astype(BF)
    ks = ksf.astype(BF)
    rs_out[...] = rs
    ks_out[...] = ks
    zero = jnp.zeros((), F32)
    v_high = jnp.where(lo, zero, kvf).astype(BF)
    v_low = jnp.where(lo, turned, zero).astype(BF)
    gains = [chunk_gain(pq, j) for j in range(8)]
    starts = [half_roll(g) for g in gains]

    t = lax.broadcasted_iota(jnp.int32, (GRP, GRP), 0)
    s = lax.broadcasted_iota(jnp.int32, (GRP, GRP), 1)
    same = t // CH == s // CH
    fine = t // 16 == s // 16
    lane = lax.broadcasted_iota(jnp.int32, (16, 128), 1)
    sub = lax.broadcasted_iota(jnp.int32, (16, 128), 0)
    eye16 = (lane % 16 == sub).astype(F32)

    rhs_all, n_all, packed = [], [], []
    for back in (False, True):
        u_dir = jnp.where(lo, zero, us) if back else jnp.where(lo, us, zero)
        ub = u_dir.astype(BF)
        strict = same & ((s > t) if back else (s < t))
        for g in range(2):
            rows = slice(g * GRP, g * GRP + GRP)
            n = jnp.where(strict, dot_nt(ub[rows], rs[rows]), zero)
            a = jnp.where(strict, dot_nt(ub[rows], ks[rows]), zero).astype(BF)
            first = jnp.concatenate(
                [u_dir[g * GRP + q * CH : g * GRP + q * CH + CH] * starts[g * 4 + q] for q in range(4)],
                axis=0,
            )
            rhs = first + dot(a, (v_low if back else v_high)[rows])
            rhs_all.append(rhs.astype(BF))
            n_all.append(jnp.where(fine, zero, n).astype(BF))
            for tile in range(2):
                acc = jnp.zeros((16, 128), F32)
                for i in range(8):
                    b = tile * 8 + i
                    acc = acc + jnp.where(
                        lane // 16 == i, n[b * 16 : b * 16 + 16, tile * 128 : tile * 128 + 128], zero
                    )
                packed.append(acc)
    solved = []
    for back in (False, True):
        tiles = packed[4 * back : 4 * back + 4]
        inv = [eye16] * 4
        for step in range(15):
            m = 15 - step if back else step
            where = (lane // 16) * 16 + m
            for k in range(4):
                coef = jnp.take_along_axis(tiles[k], where, axis=1)
                inv[k] = inv[k] - coef * inv[k][m : m + 1, :]
        solved += inv
    for i in range(4):
        back, g = divmod(i, 2)
        for b in range(16):
            tile = b // 8
            piece = jnp.where(lane // 16 == b % 8, solved[2 * i + tile], zero).astype(BF)
            empty = jnp.zeros((16, 128), BF)
            xs[b * 16 : b * 16 + 16, :] = jnp.concatenate(
                [piece, empty] if tile == 0 else [empty, piece], axis=1
            )
        xd = xs[...]
        y = dot(xd, rhs_all[i])
        z = dot(xd, n_all[i]).astype(BF)
        a = y - dot(z, y.astype(BF))
        p = a + dot(z, dot(z, a.astype(BF)).astype(BF))
        resp[back, g * GRP : g * GRP + GRP, :] = p.astype(BF)

    tt = lax.broadcasted_iota(jnp.int32, (128, 128), 0)
    ss = lax.broadcasted_iota(jnp.int32, (128, 128), 1)
    eye = tt == ss
    lo2 = ss < CH
    diag = (tt < CH) == lo2
    for j in range(8):
        rows = slice(j * CH, j * CH + CH)
        gain = gains[j]
        right = jnp.concatenate([ksf[rows] * gain, rsf[rows] * (-gain)], axis=0).astype(BF)
        through = gain * starts[j]
        f = dot_tn(jnp.concatenate([v_high[rows], resp[0, rows, :]], axis=0), right)
        b = dot_tn(jnp.concatenate([v_low[rows], resp[1, rows, :]], axis=0), right)
        keep = jnp.where(eye, through, zero)
        ta[0, j] = f + keep
        ta[1, j] = b + keep
    state = eye.astype(F32)
    for j in range(8):
        pre_out[j] = state.astype(BF)
        step = jnp.where(lo2, ta[0, j], ta[1, 7 - j])
        move = jnp.where(diag, step, zero)
        add = jnp.where(diag, zero, step)
        move_hi = move.astype(BF)
        move_lo = (move - move_hi.astype(F32)).astype(BF)
        st_hi = state.astype(BF)
        st_lo = (state - st_hi.astype(F32)).astype(BF)
        left = jnp.concatenate([st_hi, st_lo], axis=1)
        state = dot(left, jnp.concatenate([move_hi, move_hi], axis=0)) + dot(st_hi, move_lo) + add
    top, bottom = state[:CH], state[CH:]
    lo3 = low_lanes((CH, 128))
    forward = jnp.where(lo3, top, half_roll(bottom)).astype(BF)
    backward = jnp.where(lo3, half_roll(top), bottom).astype(BF)
    for d in range(8):
        send[d] = jnp.where(d > idx[0], forward, backward)


def maps(*args):
    full = ((ROWS, 128), BF)
    return call(
        maps_body,
        [((8, CH, 128), BF), ((2, ROWS, 128), BF), full, full, full, ((8, 128, 128), BF)],
        1,
        6,
        [pltpu.VMEM((GRP, GRP), BF), pltpu.VMEM((2, 8, 128, 128), F32)],
        flops=2 * ROWS * 2048 * 128 + 16 * 2 * 256**3,
        name="maps",
    )(*args)


def reads_body(normed, wq, pq, resp, rs, ks, kv, pre, thr_out, own_out):
    qq = dot(normed[...], wq[:, 0:128]).astype(BF).astype(F32)
    lo = low_lanes((ROWS, 128))
    zero = jnp.zeros((), F32)
    qs = qq * pq[...]
    kvf = kv[...].astype(F32)
    v_high = jnp.where(lo, zero, kvf).astype(BF)
    v_low = jnp.where(lo, half_roll(kvf), zero).astype(BF)
    t = lax.broadcasted_iota(jnp.int32, (GRP, GRP), 0)
    s = lax.broadcasted_iota(jnp.int32, (GRP, GRP), 1)
    same = t // CH == s // CH
    lo_c = low_lanes((CH, 128))
    full = [[], []]
    for back in (False, True):
        q_dir = jnp.where(lo, zero, qs) if back else jnp.where(lo, qs, zero)
        qb = q_dir.astype(BF)
        incl = same & ((s >= t) if back else (s <= t))
        v_dir = v_low if back else v_high
        for g in range(2):
            rows = slice(g * GRP, g * GRP + GRP)
            ar = jnp.where(incl, dot_nt(qb[rows], rs[rows, :]), zero).astype(BF)
            ak = jnp.where(incl, dot_nt(qb[rows], ks[rows, :]), zero).astype(BF)
            part = dot(ak, v_dir[rows]) - dot(ar, resp[int(back), rows, :])
            for c in range(4):
                j = g * 4 + c
                gain = half_roll(chunk_gain(pq, j))
                piece = part[c * CH : c * CH + CH]
                from_q = q_dir[j * CH : j * CH + CH] * gain
                keep = jnp.where(lo_c, zero, piece) if not back else jnp.where(lo_c, piece, zero)
                thr = (piece - keep + from_q).astype(BF)
                slot = 7 - j if back else j
                full[back].append(dot_nt(thr, pre[slot]) + keep)
    fwd = jnp.concatenate(full[0], axis=0)
    bwd = jnp.concatenate(full[1], axis=0)
    thr_out[...] = jnp.where(lo, fwd, bwd).astype(BF)
    own = jnp.where(lo, bwd, fwd)
    own_out[...] = own + half_roll(own)


def reads(*args):
    return call(
        reads_body,
        [((ROWS, 128), BF), ((ROWS, 128), F32)],
        0,
        8,
        flops=2 * ROWS * 2048 * 128 + 8 * 2 * 256**3,
        name="reads",
    )(*args)


def finish_body(idx, recv, s0, thr, own, scale, o0, o1, o2, o3, mixed):
    z, x = idx[0], idx[1]
    lo = low_lanes((CH, 128))
    state = s0[...]
    zero = jnp.zeros((), F32)
    for i in range(7):
        f = recv[i].astype(F32)
        b = recv[7 - i].astype(F32)
        move = jnp.concatenate([jnp.where(lo, f, zero), jnp.where(lo, zero, b)], axis=0).astype(BF)
        add = half_roll(jnp.where(lo, b, f))
        st_hi = state.astype(BF)
        st_lo = (state - st_hi.astype(F32)).astype(BF)
        new = dot(jnp.concatenate([st_hi, st_lo], axis=1), jnp.concatenate([move, move], axis=0)) + add
        use_f = i < z
        use_b = 7 - i > z
        use = jnp.where(lo, use_f.astype(jnp.int32), use_b.astype(jnp.int32)) > 0
        state = jnp.where(use, new, state)
    total = dot_nt(thr[...], state.astype(BF)) + own[:, :CH]
    centered = total - jnp.mean(total, axis=1, keepdims=True)
    scaled = centered * lax.rsqrt(jnp.mean(centered * centered, axis=1, keepdims=True) + 0.00064)
    mixed[...] = (scaled * scale[...]).astype(BF)
    for shift, o in zip(SHIFTS, (o0, o1, o2, o3)):
        row0 = pl.multiple_of(lax.rem(x + shift + 4, 4) * 128, 128)
        o[...] = mixed[pl.ds(row0, 128), :]


def finish(*args):
    return call(
        finish_body,
        [((128, CH), BF)] * 4,
        1,
        5,
        [pltpu.VMEM((ROWS, CH), BF)],
        flops=10**8,
        name="finish",
    )(*args)


def glu_body(normed, wg, glu, top, bottom):
    both = dot(normed[...], wg[:, 128:384])
    g = (both[:, :128] * jax.nn.sigmoid(both[:, 128:])).astype(BF)
    glu[...] = g
    top[...] = g[:16]
    bottom[...] = g[ROWS - 16 :]


def gated(*args):
    return call(
        glu_body,
        [((ROWS, 128), BF), ((16, 128), BF), ((16, 128), BF)],
        0,
        2,
        flops=2 * ROWS * 2048 * 256,
        name="gated",
    )(*args)


def conv_body(idx, glu, low, high, taps, o0, o1, o2, o3, pad, out):
    x = idx[1]
    pad[0:16, :] = low[...].astype(F32)
    pad[16 : 16 + ROWS, :] = glu[...].astype(F32)
    pad[16 + ROWS : 32 + ROWS, :] = high[...].astype(F32)

    def tile(i, carry):
        base = pl.multiple_of(i * 64, 64)
        acc = jnp.zeros((64, 128), F32)
        for j in range(31):
            acc = acc + taps[j : j + 1, :] * pad[pl.ds(base + j + 1, 64), :]
        out[pl.ds(base, 64), :] = acc.astype(BF)
        return carry

    lax.fori_loop(0, ROWS // 64, tile, 0)
    for shift, o in zip(SHIFTS, (o0, o1, o2, o3)):
        row0 = pl.multiple_of(lax.rem(x + shift + 4, 4) * 128, 128)
        o[...] = out[pl.ds(row0, 128), :]


def conv(*args):
    return call(
        conv_body,
        [((128, 128), BF)] * 4,
        1,
        4,
        [pltpu.VMEM((ROWS + 32, 128), F32), pltpu.VMEM((ROWS, 128), BF)],
        flops=2 * ROWS * 128 * 31 * 8,
        name="conv",
    )(*args)


def stats_body(idx, c0, c1, c2, c3, joined, stat):
    x = idx[1]
    first = jnp.zeros((128, 1), F32)
    second = jnp.zeros((128, 1), F32)
    for shift, ref in zip(SHIFTS, (c0, c1, c2, c3)):
        at = pl.multiple_of(lax.rem(x - shift + 4, 4) * 128, 128)
        block = ref[...]
        joined[:, pl.ds(at, 128)] = block
        wide = block.astype(F32)
        first = first + jnp.sum(wide, axis=1, keepdims=True)
        second = second + jnp.sum(wide * wide, axis=1, keepdims=True)
    lane = lax.broadcasted_iota(jnp.int32, (128, 128), 1)
    stat[...] = jnp.where(lane == 0, first, second)


def stats(*args):
    return call(
        stats_body, [((128, 512), BF), ((128, 128), F32)], 1, 4, flops=10**6, name="stats"
    )(*args)


def assemble_body(idx, w0, w1, w2, w3, out):
    y = idx[2]
    for shift, w in zip(SHIFTS, (w0, w1, w2, w3)):
        at = pl.multiple_of(lax.rem(y - shift + 4, 4) * 16, 16)
        out[:, pl.ds(at, 16), :] = w[...]


def assemble(*args):
    return call(assemble_body, [((32, 64, 768), BF)], 1, 4, flops=10**6, name="assemble")(*args)[0]


def conv_out_body(joined, mine, theirs, scale, w, part):
    conv = joined[...].astype(F32)
    total = mine[...] + theirs[...]
    mean = total[:, 0:1] * (1.0 / 1024)
    power = total[:, 1:2] * (1.0 / 1024) - mean * mean
    normed = (conv - mean) * lax.rsqrt(power + 1e-05) * scale[...]
    act = (normed * jax.nn.sigmoid(normed)).astype(BF)
    part[...] = dot_nt(act, w[:, 256:768])


def conv_out(*args):
    return call(
        conv_out_body, [((128, 2048), F32)], 0, 5, flops=2 * 128 * 512 * 2048, name="conv_out"
    )(*args)[0]


def mixer_out_body(idx, m0, m1, m2, m3, part, w, own, send, rows, total):
    x, c = idx[1], idx[3]
    for shift, ref in zip(SHIFTS, (m0, m1, m2, m3)):
        rows[lax.rem(x - shift + 4, 4)] = ref[...]
    act = jnp.concatenate([rows[0], rows[1], rows[2], rows[3]], axis=1)
    total[...] = part[...] + dot_nt(act, w[:, 0:256])
    own[...] = total[pl.ds(pl.multiple_of(c * 64, 64), 64), :]
    send[...] = total[pl.ds(pl.multiple_of((1 - c) * 64, 64), 64), :].astype(BF)


def mixer_out(*args):
    return call(
        mixer_out_body,
        [((64, 2048), F32), ((64, 2048), BF)],
        1,
        6,
        [pltpu.VMEM((4, 128, CH), BF), pltpu.VMEM((128, 2048), F32)],
        flops=2 * 128 * 256 * 2048,
        name="mixer_out",
    )(*args)


def ring(axis, shift):
    n = lax.axis_size(axis)
    return [(i, (i + shift) % n) for i in range(n)]


def moved(a, axis, shift):
    return lax.ppermute(a, axis, ring(axis, shift))


def swapped(a):
    return lax.ppermute(a, "tp", [(0, 1), (1, 0)])


def to_all(pieces, axes):
    return lax.all_to_all(pieces, axes, 0, 0, tiled=True)


def spread(a):
    return jnp.broadcast_to(a[None], (8, *a.shape)).reshape(8 * a.shape[0], *a.shape[1:])


def per_device(
    inputs, input_norm_scale, query_matrix, key_matrix, value_matrix, decay_down_weight,
    decay_up_weight, decay_bias_base, decay_position_offset, extra_log_decay,
    correction_down_weight, correction_up_weight, correction_rate_bias, head_norm_scale,
    starting_states, pointwise_value_weight, pointwise_gate_weight, depthwise_taps_weight,
    channel_norm_scale, mixer_output_weight, convolution_output_weight,
):
    z, x = lax.axis_index("z"), lax.axis_index("x")
    y, c = lax.axis_index("fs"), lax.axis_index("tp")
    idx = jnp.stack([z, x, y, c]).astype(jnp.int32)

    own = inputs[0]
    blocks = [own] + [moved(own, "x", s) for s in SHIFTS[1:]]
    far = [swapped(b) for b in blocks]
    marks = jnp.concatenate([decay_position_offset[0].T, extra_log_decay[0].T], axis=0)
    marks = [marks] + [moved(marks, "x", s) for s in SHIFTS[1:]]

    def heads(w):
        return w.reshape(64, 4, -1).transpose(1, 0, 2)

    wkv = to_all(
        spread(jnp.concatenate([heads(key_matrix), heads(value_matrix)], axis=2)), ("z", "x")
    ).reshape(2048, 128)
    wq = heads(query_matrix)
    late = to_all(
        spread(
            jnp.concatenate(
                [wq, wq, heads(pointwise_value_weight), heads(pointwise_gate_weight)], axis=2
            )
        ),
        ("z", "x"),
    ).reshape(2048, 384)
    quarter = jnp.concatenate(
        [
            lax.dynamic_slice_in_dim(mixer_output_weight, y * 16, 16, 1),
            lax.dynamic_slice_in_dim(convolution_output_weight, y * 16, 16, 1),
        ],
        axis=0,
    ).T
    wide = to_all(jnp.broadcast_to(quarter[None], (32, 16, 768)), ("z", "x"))

    def my_head(w, width=CH):
        return lax.dynamic_slice_in_dim(w, x * width, width, w.ndim - 1)

    def twice(w):
        return jnp.concatenate([w, w], axis=-1)

    normed, pu, pr, pq, rate = prepare(
        idx, *blocks, *far, *marks, input_norm_scale.reshape(2, 1024), decay_down_weight,
        correction_down_weight, twice(my_head(decay_up_weight)), twice(my_head(correction_up_weight)),
        twice(my_head(decay_bias_base))[None], twice(my_head(correction_rate_bias))[None],
    )
    send, resp, rs, ks, kv, pre = maps(idx, normed, wkv, pu, pr, pq, rate)
    states = to_all(send, ("z",))
    thr, rest = reads(normed, late, pq, resp, rs, ks, kv, pre)

    glu, top, bottom = gated(normed, late)
    low = lax.ppermute(bottom, "z", [(i, i + 1) for i in range(7)])
    high = lax.ppermute(top, "z", [(i + 1, i) for i in range(7)])
    sent = conv(idx, glu, low, high, my_head(depthwise_taps_weight, 128))
    convs = [sent[0]] + [moved(b, "x", s) for b, s in zip(sent[1:], SHIFTS[1:])]
    joined, stat = stats(idx, *convs)
    out_weights = assemble(idx, wide, *[moved(wide, "fs", s) for s in SHIFTS[1:]]).reshape(2048, 768)
    part = conv_out(joined, stat, swapped(stat), channel_norm_scale[None], out_weights)

    first = lax.dynamic_index_in_dim(starting_states[0], x, 1, False)
    first = jnp.concatenate([first[0], first[1]], axis=1)
    mixed = finish(idx, states, first, thr, rest, my_head(head_norm_scale)[None])
    mixes = [mixed[0]] + [moved(b, "x", s) for b, s in zip(mixed[1:], SHIFTS[1:])]
    mine, theirs = mixer_out(idx, *mixes, part, out_weights)
    return (mine + swapped(theirs).astype(F32)).astype(BF)[None]


SEQ = ("z", "x")


def solution(mesh):
    finer = Mesh(mesh.devices.reshape(8, 4, 4, 2), ("z", "x", "fs", "tp"))
    return jax.shard_map(
        per_device,
        mesh=finer,
        in_specs=(
            P("fs", SEQ, "tp"), P(), P(SEQ, "tp"), P(SEQ, "tp"), P(SEQ, "tp"), P(), P(None, "tp"),
            P("tp"), P("fs", SEQ, "tp"), P("fs", SEQ, "tp"), P(), P(None, "tp"), P("tp"), P("tp"),
            P("fs", None, "tp", None, None), P(SEQ, "tp"), P(SEQ, "tp"), P(None, "tp"), P("tp"),
            P("tp", SEQ), P("tp", SEQ),
        ),
        out_specs=P("fs", ("z", "x", "tp"), None),
        check_vma=False,
    )
```

time: 522 us -> 204 us (0.39)
  blocking collectives: 177 us -> 0 us
  matrix products: 117 us -> 0 us
  starting transfers between devices: 9.95 us -> 73.3 us
  local copies, waits for them, and re-layouts: 76.1 us -> 13.7 us
  Pallas kernels: 0 us -> 45.7 us
  other arithmetic: 48.9 us -> 5.38 us
  between operations: 14.4 us -> 0.36 us
  waiting for transfers between devices: 70.6 us -> 64.3 us
    all_gather x11 -> x0, blocking collectives: 173 us -> none  [the longest x8 122 us: carried_in(): lax.all_gather(part.astype(kind), axis)]
    dot_general x319 -> x0, matrix products: 113 us -> none  [the longest x128 36.5 us: local_step(): projected = jnp.einsum('dhvk,dhk->dhv', stacked, unit_key)]
    all_gather x2 -> x0, waiting for transfers between devices: 70.5 us -> none  [the longest x1 70.5 us: sent_together(): lax.all_gather(both, axis, axis=dim, tiled=True)]
    all_to_all x1 -> x4, waiting for transfers between devices: 0.01 us -> 54.9 us  [to_all(): return lax.all_to_all(pieces, axes, 0, 0, tiled=True)]
    slice x35 -> x0, local copies, waits for them, and re-layouts: 46.4 us -> none  [the longest x32 45.5 us: mixer_branch(): ends, emitted = lax.scan(local_step, start, steps, unroll=8)]
    pallas_call x0 -> x10, Pallas kernels: none -> 45.7 us  [the longest x1 9.03 us: maps(): call(maps_body, [((8, CH, 128), BF), ((2, ROWS, 128), BF), full, full, fu...]
    ppermute x2 -> x23, starting transfers between devices: 3.24 us -> 42 us  [the longest x15 23.6 us: moved(): return lax.ppermute(a, axis, ring(axis, shift))]
    all_to_all x1 -> x4, starting transfers between devices: 6.68 us -> 31.3 us  [to_all(): return lax.all_to_all(pieces, axes, 0, 0, tiled=True)]
  transfers between devices with their start and end apart: 5 -> 27, of which waited for: 1 -> 7; matrix products, arithmetic and copies ran while one was open for 45% -> 5% of each run, Pallas kernels for 0% -> 21%
where the time goes in v1:
time: 204 us; the launch traced here: 203 us
  starting transfers between devices  73.3 us (36%)
  waiting for transfers between devices  64.3 us (32%)
  Pallas kernels  45.7 us (22%)
  local copies, waits for them, and re-layouts  13.7 us (7%)
  other arithmetic  5.38 us (3%)
    all_to_all x4, waiting for transfers between devices, to_all(): return lax.all_to_all(pieces, axes, 0, 0, tiled=True)  54.9 us
    all_to_all x4, starting transfers between devices, to_all(): return lax.all_to_all(pieces, axes, 0, 0, tiled=True)  31.3 us
    ppermute x15, starting transfers between devices, moved(): return lax.ppermute(a, axis, ring(axis, shift))  23.6 us
    ppermute x6, starting transfers between devices, swapped(): return lax.ppermute(a, 'tp', [(0, 1), (1, 0)])  14.1 us
    pallas_call x1, Pallas kernels, maps(): call(maps_body, [((8, CH, 128), BF), ((2, ROWS, 128), BF), full, full, fu...  9.03 us
    pallas_call x1, Pallas kernels, prepare(): call(prepare_body, [((ROWS, 2048), BF), full, full, full, full], 1, 19, [...  8.84 us
    pallas_call x1, Pallas kernels, reads(): call(reads_body, [((ROWS, 128), BF), ((ROWS, 128), F32)], 0, 8, flops=2 *...  6.16 us
    ppermute x15, waiting for transfers between devices, moved(): return lax.ppermute(a, axis, ring(axis, shift))  5.7 us
  transfers between devices with their start and end apart: 27, of which 7 were waited for; matrix products, arithmetic and copies ran while one was open for 5% of the time, Pallas kernels for 21%

profile of v1, /device:TPU:1, one launch (start us, length us, event | category | flops | bytes accessed | tf_op | source)
XLA Modules:
  0.0 202.8 jit_solution(6963794174238813452)
XLA Ops:
  0.0 0.8 copy-done
  0.8 0.7 constant_dynamic-slice_fusion.1
  1.5 1.0 broadcast_in_dim.39
  2.5 11.9 %all-to-all-start.3 = ((bf16[32,16,768]{2,1,0:T(8,128)(2,1)}), bf16[32,16,768]{2,1,0:T(8,128)(2,1)S(1)}, u32[]{:S(2)}, u32[]{:S(2)}) async-start(bf16[32,16,768]{2,1,0:T(8,128)(2,1)} %broadcast_in_dim.39), calls=%async_computation.3 | async-start | bytes 1572864 | tf_op jit(solution)/shard_map/all_to_all | solution.py:482
  14.6 0.2 pad_maximum_fusion
  14.8 20.6 %all-to-all-done.3.w0 = bf16[32,16,768]{2,1,0:T(8,128)(2,1)S(1)} async-done(((bf16[32,16,768]{2,1,0:T(8,128)(2,1)}), bf16[32,16,768]{2,1,0:T(8,128)(2,1)S(1)}, u32[]{:S(2)}, u32[]{:S(2)}) %all-to-all-start.3) | async-done | bytes 786464 | tf_op jit(solution)/shard_map/all_to_all | solution.py:482
  35.5 1.5 broadcast_in_dim.36
  37.0 5.9 %all-to-all-start.2 = ((bf16[32,64,384]{2,1,0:T(8,128)(2,1)}), bf16[32,64,384]{2,1,0:T(8,128)(2,1)S(1)}, u32[]{:S(2)}, u32[]{:S(2)}) async-start(bf16[32,64,384]{2,1,0:T(8,128)(2,1)} %bitcast.20), calls=%async_computation.2 | async-start | bytes 3145728 | tf_op jit(solution)/shard_map/all_to_all | solution.py:482
  42.9 1.3 collective-permute-start
  44.6 34.2 %all-to-all-done.2 = bf16[32,64,384]{2,1,0:T(8,128)(2,1)S(1)} async-done(((bf16[32,64,384]{2,1,0:T(8,128)(2,1)}), bf16[32,64,384]{2,1,0:T(8,128)(2,1)S(1)}, u32[]{:S(2)}, u32[]{:S(2)}) %all-to-all-start.2) | async-done | bytes 1572896 | tf_op jit(solution)/shard_map/all_to_all | solution.py:482
  78.8 1.0 broadcast_in_dim.35
  79.9 7.3 %all-to-all-start = ((bf16[32,64,128]{2,1,0:T(8,128)(2,1)}), bf16[32,64,128]{2,1,0:T(8,128)(2,1)S(1)}, u32[]{:S(2)}, u32[]{:S(2)}) async-start(bf16[32,64,128]{2,1,0:T(8,128)(2,1)} %bitcast.13), calls=%async_computation | async-start | bytes 1048576 | tf_op jit(solution)/shard_map/all_to_all | solution.py:482
  87.1 2.5 %collective-permute-start.1 = (bf16[128,1024]{1,0:T(8,128)(2,1)S(1)}, bf16[128,1024]{1,0:T(8,128)(2,1)}, u32[]{:S(2)}, u32[]{:S(2)}) collective-permute-start(bf16[128,1024]{1,0:T(8,128)(2,1)S(1)} %bitcast.43), channel_id=1, source_target_pairs={{0,24},{8,0},{16,8},{24,16},{1,25},{9,1},{17,9},{25,17},{2,26},{10... | collective-permute-start | bytes 786440 | tf_op jit(solution)/shard_map/ppermute | solution.py:474
  89.7 0.6 collective-permute-start.2
  90.2 3.5 %collective-permute-start.3 = (bf16[128,1024]{1,0:T(8,128)(2,1)S(1)}, bf16[128,1024]{1,0:T(8,128)(2,1)}, u32[]{:S(2)}, u32[]{:S(2)}) collective-permute-start(bf16[128,1024]{1,0:T(8,128)(2,1)S(1)} %bitcast.45), channel_id=1, source_target_pairs={{0,1},{1,0},{2,3},{3,2},{4,5},{5,4},{6,7},{7,6},{8,9},{9,8},{10,11... | collective-permute-start | bytes 786440 | tf_op jit(solution)/shard_map/ppermute | solution.py:478
  93.8 0.7 collective-permute-start.7
  94.4 0.3 collective-permute-start.4
  94.7 0.9 constant_dynamic-slice_fusion.3
  95.6 2.8 %collective-permute-done.7.m1 = f32[8,128]{1,0:T(8,128)S(1)} collective-permute-done((f32[8,128]{1,0:T(8,128)S(1)}, f32[8,128]{1,0:T(8,128)S(1)}, u32[]{:S(2)}, u32[]{:S(2)}) %collective-permute-start.7) | collective-permute-done | bytes 4128 | tf_op jit(solution)/shard_map/ppermute | solution.py:474
  98.4 4.3 %collective-permute-start.8 = (f32[8,128]{1,0:T(8,128)S(1)}, f32[8,128]{1,0:T(8,128)S(1)}, u32[]{:S(2)}, u32[]{:S(2)}) collective-permute-start(f32[8,128]{1,0:T(8,128)S(1)} %pad_maximum_fusion.5.m0), channel_id=1, source_target_pairs={{0,24},{8,0},{16,8},{24,16},{1,25},{9,1},{17,9},{25,17},{2,26},{10... | collective-permute-start | bytes 12296 | tf_op jit(solution)/shard_map/ppermute | solution.py:474
  102.7 0.7 pad_maximum_fusion.2.dup
  103.5 0.4 collective-permute-done.8.m2
  104.0 2.8 %collective-permute-start.9 = (f32[8,128]{1,0:T(8,128)S(1)}, f32[8,128]{1,0:T(8,128)S(1)}, u32[]{:S(2)}, u32[]{:S(2)}) collective-permute-start(f32[8,128]{1,0:T(8,128)S(1)} %pad_maximum_fusion.5.m0), channel_id=1, source_target_pairs={{0,16},{8,24},{16,0},{24,8},{1,17},{9,25},{17,1},{25,9},{2,18},{10... | collective-permute-start | bytes 12296 | tf_op jit(solution)/shard_map/ppermute | solution.py:474
  106.8 0.7 maximum_bitcast_fusion.1
  107.5 3.1 %collective-permute-start.5 = (bf16[128,1024]{1,0:T(8,128)(2,1)}, bf16[128,1024]{1,0:T(8,128)(2,1)}, u32[]{:S(2)}, u32[]{:S(2)}) collective-permute-start(bf16[128,1024]{1,0:T(8,128)(2,1)} %collective-permute-done.1.a2), channel_id=1, source_target_pairs={{0,1},{1,0},{2,3},{3,2},{4,5},{5,4},{6,7},{7,6},{8,9},{9,8},{10,11... | collective-permute-start | bytes 786440 | tf_op jit(solution)/shard_map/ppermute | solution.py:478
  110.7 1.3 collective-permute-start.19
  112.0 1.5 collective-permute-start.20
  113.5 1.6 collective-permute-start.21
  115.1 0.6 pad_add_fusion.idx
  115.6 0.6 reshape.42.scale
  116.2 0.7 pad_maximum_fusion.3.cup
  116.9 0.8 dynamic-slice_bitcast_fusion.1
  117.8 8.8 %prepare.1 = (bf16[512,2048]{1,0:T(8,128)(2,1)}, f32[512,128]{1,0:T(8,128)}, f32[512,128]{1,0:T(8,128)}, f32[512,128]{1,0:T(8,128)}, f32[512,128]{1,0:T(8,128)}) custom-call(s32[4]{0:T(128)} %pad_add_fusion.idx, bf16[128,1024]{1,0:T(8,128)(2,1)} %bitcast.41, bf16[128,1024]{1,0:T(8,128)(2,1)} %copy-done.6, bf16[128,1024]{1,0:T(8,128)(2,1)} %collective-permute-done.1.a2, ...), custom_call_target="tpu_custom_call" | custom-call | flops 536870912 | tf_op jit(solution)/shard_map/prepare/pallas_call | solution.py:113
  126.6 3.4 %gated.1 = (bf16[512,128]{1,0:T(8,128)(2,1)}, bf16[16,128]{1,0:T(8,128)(2,1)}, bf16[16,128]{1,0:T(8,128)(2,1)}) custom-call(bf16[512,2048]{1,0:T(8,128)(2,1)} %get-tuple-element.33.normed, bf16[2048,384]{1,0:T(8,128)(2,1)} %bitcast.38), custom_call_target="tpu_custom_call" | custom-call | flops 536870912 | tf_op jit(solution)/shard_map/gated/pallas_call | solution.py:356
  130.0 3.1 %collective-permute-start.13 = (bf16[16,128]{1,0:T(8,128)(2,1)}, bf16[16,128]{1,0:T(8,128)(2,1)S(1)}, u32[]{:S(2)}, u32[]{:S(2)}) collective-permute-start(bf16[16,128]{1,0:T(8,128)(2,1)} %get-tuple-element.51), channel_id=1, source_target_pairs={{0,32},{32,64},{64,96},{96,128},{128,160},{160,192},{192,224},{1,3... | collective-permute-start | bytes 12296 | tf_op jit(solution)/shard_map/ppermute | solution.py:546
  133.1 1.3 collective-permute-start.14
  134.4 1.3 constant_dynamic-slice_fusion.2.taps
  135.8 2.3 %collective-permute-done.14.high = bf16[16,128]{1,0:T(8,128)(2,1)S(1)} collective-permute-done((bf16[16,128]{1,0:T(8,128)(2,1)}, bf16[16,128]{1,0:T(8,128)(2,1)S(1)}, u32[]{:S(2)}, u32[]{:S(2)}) %collective-permute-start.14) | collective-permute-done | bytes 4128 | tf_op jit(solution)/shard_map/ppermute | solution.py:547
  138.1 0.6 copy-done.25
  138.7 2.3 %conv.1 = (bf16[128,128]{1,0:T(8,128)(2,1)}, bf16[128,128]{1,0:T(8,128)(2,1)}, bf16[128,128]{1,0:T(8,128)(2,1)}, bf16[128,128]{1,0:T(8,128)(2,1)}) custom-call(s32[4]{0:T(128)} %pad_add_fusion.idx, bf16[512,128]{1,0:T(8,128)(2,1)} %get-tuple-element.50.glu, bf16[16,128]{1,0:T(8,128)(2,1)} %copy-done.24, bf16[16,128]{1,0:T(8,128)(2,1)} %copy-done.25, ...), custom_call_target="tpu_custom_call" | custom-call | flops 32505856 | tf_op jit(solution)/shard_map/conv/pallas_call | solution.py:387
  141.0 1.2 collective-permute-start.15
  142.2 0.8 copy-done.3
  143.0 9.0 %maps.1 = (bf16[8,64,128]{2,1,0:T(8,128)(2,1)}, bf16[2,512,128]{2,1,0:T(8,128)(2,1)}, bf16[512,128]{1,0:T(8,128)(2,1)}, bf16[512,128]{1,0:T(8,128)(2,1)}, bf16[5...) custom-call(s32[4]{0:T(128)} %pad_add_fusion.idx, bf16[512,2048]{1,0:T(8,128)(2,1)} %get-tuple-element.33.normed, ...), custom_call_target="tpu_custom_call" | custom-call | flops 805306368 | tf_op jit(solution)/shard_map/maps/pallas_call | solution.py:248
  152.0 6.3 %all-to-all-start.1 = ((bf16[8,64,128]{2,1,0:T(8,128)(2,1)}), bf16[8,64,128]{2,1,0:T(8,128)(2,1)S(1)}, u32[]{:S(2)}, u32[]{:S(2)}) async-start(bf16[8,64,128]{2,1,0:T(8,128)(2,1)} %get-tuple-element.38), calls=%async_computation.1 | async-start | bytes 262144 | tf_op jit(solution)/shard_map/all_to_all | solution.py:482
  158.3 1.9 collective-permute-start.16
  160.2 1.3 collective-permute-start.17
  161.4 0.7 pad_maximum_fusion.4.s0
  162.1 2.4 %collective-permute-done.17.c3 = bf16[128,128]{1,0:T(8,128)(2,1)S(1)} collective-permute-done((bf16[128,128]{1,0:T(8,128)(2,1)S(1)}, bf16[128,128]{1,0:T(8,128)(2,1)S(1)}, u32[]{:S(2)}, u32[]{:S(2)}) %collective-permute-start.17) | collective-permute-done | bytes 32800 | tf_op jit(solution)/shard_map/ppermute | solution.py:474
  164.5 0.6 copy-done.18
  165.1 1.7 stats.1
  166.8 5.5 %collective-permute-start.18 = (f32[128,128]{1,0:T(8,128)}, f32[128,128]{1,0:T(8,128)S(1)}, u32[]{:S(2)}, u32[]{:S(2)}) collective-permute-start(f32[128,128]{1,0:T(8,128)} %get-tuple-element.58.mine), channel_id=1, source_target_pairs={{0,1},{1,0},{2,3},{3,2},{4,5},{5,4},{6,7},{7,6},{8,9},{9,8},{10,11... | collective-permute-start | bytes 196616 | tf_op jit(solution)/shard_map/ppermute | solution.py:478
  172.3 0.6 dynamic-slice_bitcast_fusion.2.scale
  172.9 3.7 %assemble.1 = bf16[32,64,768]{2,1,0:T(8,128)(2,1)} custom-call(s32[4]{0:T(128)} %pad_add_fusion.idx, bf16[32,16,768]{2,1,0:T(8,128)(2,1)} %copy-done.2, bf16[32,16,768]{2,1,0:T(8,128)(2,1)} %collective-permute-done.19.w1, bf16[32,16,768]{2,1,0:T(8,128)(2,1)} %collective-permute-done.20.w2, bf16[32,16,768]{2,1,0:T(8,128)(2,1)} %collective-permute-done.21.w3), custom_call_target="tpu_custom_call" | custom-call | flops 1000000 | tf_op jit(solution)/shard_map/assemble/pallas_call | solution.py:427
  176.6 6.2 %reads.1 = (bf16[512,128]{1,0:T(8,128)(2,1)}, f32[512,128]{1,0:T(8,128)}) custom-call(bf16[512,2048]{1,0:T(8,128)(2,1)} %get-tuple-element.33.normed, bf16[2048,384]{1,0:T(8,128)(2,1)} %bitcast.39, f32[512,128]{1,0:T(8,128)} %get-tuple-element.36.pq, bf16[2,512,128]{2,1,0:T(8,128)(2,1)} %get-tuple-element.39.resp, bf16[512,128]{1,0:T(8,128)(2,1)} %get-tuple-element.40.rs, ...), custom_call_target="tpu_custom_call" | custom-call | flops 536870912 | tf_op jit(solution)/shard_map/reads/pallas_call | solution.py:299
  182.8 0.7 copy-done.4
  183.4 3.0 %finish.1 = (bf16[128,64]{1,0:T(8,128)(2,1)}, bf16[128,64]{1,0:T(8,128)(2,1)}, bf16[128,64]{1,0:T(8,128)(2,1)}, bf16[128,64]{1,0:T(8,128)(2,1)}) custom-call(s32[4]{0:T(128)} %pad_add_fusion.idx, bf16[8,64,128]{2,1,0:T(8,128)(2,1)} %copy-done.4, f32[64,128]{1,0:T(8,128)} %pad_maximum_fusion.4.s0, bf16[512,128]{1,0:T(8,128)(2,1)} %get-tuple-element.44.thr, ...), custom_call_target="tpu_custom_call" | custom-call | flops 100000000 | tf_op jit(solution)/shard_map/finish/pallas_call | solution.py:336
  186.5 2.7 %collective-permute-start.11 = (bf16[128,64]{1,0:T(8,128)(2,1)}, bf16[128,64]{1,0:T(8,128)(2,1)S(1)}, u32[]{:S(2)}, u32[]{:S(2)}) collective-permute-start(bf16[128,64]{1,0:T(8,128)(2,1)} %get-tuple-element.48), channel_id=1, source_target_pairs={{0,24},{8,0},{16,8},{24,16},{1,25},{9,1},{17,9},{25,17},{2,26},{10... | collective-permute-start | bytes 49160 | tf_op jit(solution)/shard_map/ppermute | solution.py:474
  189.1 0.6 copy-done.7
  189.8 4.0 %conv_out.1.part = f32[128,2048]{1,0:T(8,128)} custom-call(bf16[128,512]{1,0:T(8,128)(2,1)} %get-tuple-element.57.joined, f32[128,128]{1,0:T(8,128)} %get-tuple-element.58.mine, f32[128,128]{1,0:T(8,128)} %copy-done.7, f32[1,512]{1,0:T(1,128)} %bitcast.51, bf16[2048,768]{1,0:T(8,128)(2,1)} %bitcast.36), custom_call_target="tpu_custom_call" | custom-call | flops 268435456 | tf_op jit(solution)/shard_map/conv_out/pallas_call | solution.py:441
  193.8 0.6 copy-done.10
  194.4 3.7 %mixer_out.1 = (f32[64,2048]{1,0:T(8,128)}, bf16[64,2048]{1,0:T(8,128)(2,1)}) custom-call(s32[4]{0:T(128)} %pad_add_fusion.idx, bf16[128,64]{1,0:T(8,128)(2,1)} %get-tuple-element.46.m0, bf16[128,64]{1,0:T(8,128)(2,1)} %copy-done.10, bf16[128,64]{1,0:T(8,128)(2,1)} %copy-done.11, bf16[128,64]{1,0:T(8,128)(2,1)} %copy-done.12, f32[128,2048]{1,0:T(8,128)} %conv_out.1.part, ...), custom_call_target="tpu_custom_call" | custom-call | flops 134217728 | tf_op jit(solution)/shard_map/mixer_out/pallas_call | solution.py:457
  198.1 1.6 collective-permute-start.22
  199.7 1.4 collective-permute-done.22
  201.0 1.8 fusion
  (95 shorter events, 0.9 us)
Async XLA Ops:
  0.0 0.8 copy-start
  0.0 14.4 %copy-start.8 = (bf16[64,512]{1,0:T(8,128)(2,1)S(1)}, bf16[64,512]{1,0:T(8,128)(2,1)}, u32[]{:S(2)}) copy-start(bf16[64,512]{1,0:T(8,128)(2,1)} %param.37) | copy-start | bytes 196612
  0.0 14.4 %copy-start.9 = (bf16[64,512]{1,0:T(8,128)(2,1)S(1)}, bf16[64,512]{1,0:T(8,128)(2,1)}, u32[]{:S(2)}) copy-start(bf16[64,512]{1,0:T(8,128)(2,1)} %param.36) | copy-start | bytes 196612
  0.0 14.5 %copy-start.13 = (bf16[64,256]{1,0:T(8,128)(2,1)S(1)}, bf16[64,256]{1,0:T(8,128)(2,1)}, u32[]{:S(2)}) copy-start(bf16[64,256]{1,0:T(8,128)(2,1)} %param.23) | copy-start | bytes 98308
  2.5 32.9 %all-to-all-start.3 = ((bf16[32,16,768]{2,1,0:T(8,128)(2,1)}), bf16[32,16,768]{2,1,0:T(8,128)(2,1)S(1)}, u32[]{:S(2)}, u32[]{:S(2)}) async-start(bf16[32,16,768]{2,1,0:T(8,128)(2,1)} %broadcast_in_dim.39), calls=%async_computation.3 | async-start | bytes 1572864 | tf_op jit(solution)/shard_map/all_to_all | solution.py:482
  14.8 28.1 %copy-start.5 = (bf16[1,128,1024]{2,1,0:T(8,128)(2,1)S(1)}, bf16[1,128,1024]{2,1,0:T(8,128)(2,1)}, u32[]{:S(2)}) copy-start(bf16[1,128,1024]{2,1,0:T(8,128)(2,1)} %param.21) | copy-start | bytes 786436
  14.8 29.4 %copy-start.14 = (bf16[64,256]{1,0:T(8,128)(2,1)S(1)}, bf16[64,256]{1,0:T(8,128)(2,1)}, u32[]{:S(2)}) copy-start(bf16[64,256]{1,0:T(8,128)(2,1)} %param.25) | copy-start | bytes 98308
  14.8 29.5 %copy-start.15 = (bf16[64,256]{1,0:T(8,128)(2,1)S(1)}, bf16[64,256]{1,0:T(8,128)(2,1)}, u32[]{:S(2)}) copy-start(bf16[64,256]{1,0:T(8,128)(2,1)} %param.24) | copy-start | bytes 98308
  35.5 78.0 %copy-start.2 = (bf16[32,16,768]{2,1,0:T(8,128)(2,1)}, bf16[32,16,768]{2,1,0:T(8,128)(2,1)S(1)}, u32[]{:S(2)}) copy-start(bf16[32,16,768]{2,1,0:T(8,128)(2,1)S(1)} %all-to-all-done.3.w0) | copy-start | bytes 2359300
  37.0 56.8 %copy-start.26 = (f32[1,128,4]{1,2,0:T(4,128)S(1)}, f32[1,128,4]{1,2,0:T(4,128)}, u32[]{:S(2)}) copy-start(f32[1,128,4]{1,2,0:T(4,128)} %param.30) | copy-start | bytes 6148
  37.0 56.8 %copy-start.27 = (f32[1,128,4]{1,2,0:T(4,128)S(1)}, f32[1,128,4]{1,2,0:T(4,128)}, u32[]{:S(2)}) copy-start(f32[1,128,4]{1,2,0:T(4,128)} %param.29) | copy-start | bytes 6148
  37.0 66.4 %copy-start.30 = (f32[256]{0:T(256)S(1)}, f32[256]{0:T(256)}, u32[]{:S(2)}) copy-start(f32[256]{0:T(256)} %param.28) | copy-start | bytes 3076
  37.0 66.5 %copy-start.31 = (f32[256]{0:T(256)S(1)}, f32[256]{0:T(256)}, u32[]{:S(2)}) copy-start(f32[256]{0:T(256)} %param.33) | copy-start | bytes 3076
  37.0 78.7 %copy-start.20 = (f32[2048]{0:T(1024)S(1)}, f32[2048]{0:T(1024)}, u32[]{:S(2)}) copy-start(f32[2048]{0:T(1024)} %param.22) | copy-start | bytes 24580
  37.0 41.8 %all-to-all-start.2 = ((bf16[32,64,384]{2,1,0:T(8,128)(2,1)}), bf16[32,64,384]{2,1,0:T(8,128)(2,1)S(1)}, u32[]{:S(2)}, u32[]{:S(2)}) async-start(bf16[32,64,384]{2,1,0:T(8,128)(2,1)} %bitcast.20), calls=%async_computation.2 | async-start | bytes 3145728 | tf_op jit(solution)/shard_map/all_to_all | solution.py:482
  42.9 51.5 %collective-permute-start = (bf16[128,1024]{1,0:T(8,128)(2,1)S(1)}, bf16[128,1024]{1,0:T(8,128)(2,1)S(1)}, u32[]{:S(2)}, u32[]{:S(2)}) collective-permute-start(bf16[128,1024]{1,0:T(8,128)(2,1)S(1)} %bitcast.42), channel_id=1, source_target_pairs={{0,8},{8,16},{16,24},{24,0},{1,9},{9,17},{17,25},{25,1},{2,10},{10... | collective-permute-start | bytes 786440 | tf_op jit(solution)/shard_map/ppermute | solution.py:474
  78.8 47.8 %copy-start.1 = (bf16[32,64,384]{2,1,0:T(8,128)(2,1)}, bf16[32,64,384]{2,1,0:T(8,128)(2,1)S(1)}, u32[]{:S(2)}) copy-start(bf16[32,64,384]{2,1,0:T(8,128)(2,1)S(1)} %all-to-all-done.2) | copy-start | bytes 4718596
  79.9 62.3 %all-to-all-start = ((bf16[32,64,128]{2,1,0:T(8,128)(2,1)}), bf16[32,64,128]{2,1,0:T(8,128)(2,1)S(1)}, u32[]{:S(2)}, u32[]{:S(2)}) async-start(bf16[32,64,128]{2,1,0:T(8,128)(2,1)} %bitcast.13), calls=%async_computation | async-start | bytes 1048576 | tf_op jit(solution)/shard_map/all_to_all | solution.py:482
  87.1 20.3 %collective-permute-start.1 = (bf16[128,1024]{1,0:T(8,128)(2,1)S(1)}, bf16[128,1024]{1,0:T(8,128)(2,1)}, u32[]{:S(2)}, u32[]{:S(2)}) collective-permute-start(bf16[128,1024]{1,0:T(8,128)(2,1)S(1)} %bitcast.43), channel_id=1, source_target_pairs={{0,24},{8,0},{16,8},{24,16},{1,25},{9,1},{17,9},{25,17},{2,26},{10... | collective-permute-start | bytes 786440 | tf_op jit(solution)/shard_map/ppermute | solution.py:474
  89.7 20.9 %collective-permute-start.2 = (bf16[128,1024]{1,0:T(8,128)(2,1)S(1)}, bf16[128,1024]{1,0:T(8,128)(2,1)}, u32[]{:S(2)}, u32[]{:S(2)}) collective-permute-start(bf16[128,1024]{1,0:T(8,128)(2,1)S(1)} %bitcast.44), channel_id=1, source_target_pairs={{0,16},{8,24},{16,0},{24,8},{1,17},{9,25},{17,1},{25,9},{2,18},{10... | collective-permute-start | bytes 786440 | tf_op jit(solution)/shard_map/ppermute | solution.py:474
  90.2 21.8 %collective-permute-start.3 = (bf16[128,1024]{1,0:T(8,128)(2,1)S(1)}, bf16[128,1024]{1,0:T(8,128)(2,1)}, u32[]{:S(2)}, u32[]{:S(2)}) collective-permute-start(bf16[128,1024]{1,0:T(8,128)(2,1)S(1)} %bitcast.45), channel_id=1, source_target_pairs={{0,1},{1,0},{2,3},{3,2},{4,5},{5,4},{6,7},{7,6},{8,9},{9,8},{10,11... | collective-permute-start | bytes 786440 | tf_op jit(solution)/shard_map/ppermute | solution.py:478
  93.8 24.0 %copy-start.19 = (f32[8,128]{1,0:T(8,128)}, f32[8,128]{1,0:T(8,128)S(1)}, u32[]{:S(2)}) copy-start(f32[8,128]{1,0:T(8,128)S(1)} %pad_maximum_fusion.5.m0) | copy-start | bytes 12292
  93.8 4.6 %collective-permute-start.7 = (f32[8,128]{1,0:T(8,128)S(1)}, f32[8,128]{1,0:T(8,128)S(1)}, u32[]{:S(2)}, u32[]{:S(2)}) collective-permute-start(f32[8,128]{1,0:T(8,128)S(1)} %pad_maximum_fusion.5.m0), channel_id=1, source_target_pairs={{0,8},{8,16},{16,24},{24,0},{1,9},{9,17},{17,25},{25,1},{2,10},{10... | collective-permute-start | bytes 12296 | tf_op jit(solution)/shard_map/ppermute | solution.py:474
  94.4 23.3 %copy-start.6 = (bf16[128,1024]{1,0:T(8,128)(2,1)}, bf16[128,1024]{1,0:T(8,128)(2,1)S(1)}, u32[]{:S(2)}) copy-start(bf16[128,1024]{1,0:T(8,128)(2,1)S(1)} %collective-permute-done.a1) | copy-start | bytes 786436
  94.4 19.1 %collective-permute-start.4 = (bf16[128,1024]{1,0:T(8,128)(2,1)S(1)}, bf16[128,1024]{1,0:T(8,128)(2,1)}, u32[]{:S(2)}, u32[]{:S(2)}) collective-permute-start(bf16[128,1024]{1,0:T(8,128)(2,1)S(1)} %collective-permute-done.a1), channel_id=1, source_target_pairs={{0,1},{1,0},{2,3},{3,2},{4,5},{5,4},{6,7},{7,6},{8,9},{9,8},{10,11... | collective-permute-start | bytes 786440 | tf_op jit(solution)/shard_map/ppermute | solution.py:478
  98.4 19.3 %copy-start.21 = (f32[8,128]{1,0:T(8,128)}, f32[8,128]{1,0:T(8,128)S(1)}, u32[]{:S(2)}) copy-start(f32[8,128]{1,0:T(8,128)S(1)} %collective-permute-done.7.m1) | copy-start | bytes 12292
  98.4 5.6 %collective-permute-start.8 = (f32[8,128]{1,0:T(8,128)S(1)}, f32[8,128]{1,0:T(8,128)S(1)}, u32[]{:S(2)}, u32[]{:S(2)}) collective-permute-start(f32[8,128]{1,0:T(8,128)S(1)} %pad_maximum_fusion.5.m0), channel_id=1, source_target_pairs={{0,24},{8,0},{16,8},{24,16},{1,25},{9,1},{17,9},{25,17},{2,26},{10... | collective-permute-start | bytes 12296 | tf_op jit(solution)/shard_map/ppermute | solution.py:474
  104.0 13.8 %copy-start.22 = (f32[8,128]{1,0:T(8,128)}, f32[8,128]{1,0:T(8,128)S(1)}, u32[]{:S(2)}) copy-start(f32[8,128]{1,0:T(8,128)S(1)} %collective-permute-done.8.m2) | copy-start | bytes 12292
  104.0 6.7 %collective-permute-start.9 = (f32[8,128]{1,0:T(8,128)S(1)}, f32[8,128]{1,0:T(8,128)S(1)}, u32[]{:S(2)}, u32[]{:S(2)}) collective-permute-start(f32[8,128]{1,0:T(8,128)S(1)} %pad_maximum_fusion.5.m0), channel_id=1, source_target_pairs={{0,16},{8,24},{16,0},{24,8},{1,17},{9,25},{17,1},{25,9},{2,18},{10... | collective-permute-start | bytes 12296 | tf_op jit(solution)/shard_map/ppermute | solution.py:474
  107.5 10.2 %collective-permute-start.5 = (bf16[128,1024]{1,0:T(8,128)(2,1)}, bf16[128,1024]{1,0:T(8,128)(2,1)}, u32[]{:S(2)}, u32[]{:S(2)}) collective-permute-start(bf16[128,1024]{1,0:T(8,128)(2,1)} %collective-permute-done.1.a2), channel_id=1, source_target_pairs={{0,1},{1,0},{2,3},{3,2},{4,5},{5,4},{6,7},{7,6},{8,9},{9,8},{10,11... | collective-permute-start | bytes 786440 | tf_op jit(solution)/shard_map/ppermute | solution.py:478
  110.6 7.1 %collective-permute-start.6 = (bf16[128,1024]{1,0:T(8,128)(2,1)}, bf16[128,1024]{1,0:T(8,128)(2,1)}, u32[]{:S(2)}, u32[]{:S(2)}) collective-permute-start(bf16[128,1024]{1,0:T(8,128)(2,1)} %collective-permute-done.2.a3), channel_id=1, source_target_pairs={{0,1},{1,0},{2,3},{3,2},{4,5},{5,4},{6,7},{7,6},{8,9},{9,8},{10,11... | collective-permute-start | bytes 786440 | tf_op jit(solution)/shard_map/ppermute | solution.py:478
  110.7 7.1 %copy-start.23 = (f32[8,128]{1,0:T(8,128)}, f32[8,128]{1,0:T(8,128)S(1)}, u32[]{:S(2)}) copy-start(f32[8,128]{1,0:T(8,128)S(1)} %collective-permute-done.9.m3) | copy-start | bytes 12292
  110.7 62.2 %collective-permute-start.19 = (bf16[32,16,768]{2,1,0:T(8,128)(2,1)S(1)}, bf16[32,16,768]{2,1,0:T(8,128)(2,1)}, u32[]{:S(2)}, u32[]{:S(2)}) collective-permute-start(bf16[32,16,768]{2,1,0:T(8,128)(2,1)S(1)} %all-to-all-done.3.w0), channel_id=1, source_target_pairs={{0,2},{2,4},{4,6},{6,0},{1,3},{3,5},{5,7},{7,1},{8,10},{10,12},{12... | collective-permute-start | bytes 2359304 | tf_op jit(solution)/shard_map/ppermute | solution.py:474
  112.0 60.9 %collective-permute-start.20 = (bf16[32,16,768]{2,1,0:T(8,128)(2,1)S(1)}, bf16[32,16,768]{2,1,0:T(8,128)(2,1)}, u32[]{:S(2)}, u32[]{:S(2)}) collective-permute-start(bf16[32,16,768]{2,1,0:T(8,128)(2,1)S(1)} %all-to-all-done.3.w0), channel_id=1, source_target_pairs={{0,6},{2,0},{4,2},{6,4},{1,7},{3,1},{5,3},{7,5},{8,14},{10,8},{12,... | collective-permute-start | bytes 2359304 | tf_op jit(solution)/shard_map/ppermute | solution.py:474
  113.5 59.4 %collective-permute-start.21 = (bf16[32,16,768]{2,1,0:T(8,128)(2,1)S(1)}, bf16[32,16,768]{2,1,0:T(8,128)(2,1)}, u32[]{:S(2)}, u32[]{:S(2)}) collective-permute-start(bf16[32,16,768]{2,1,0:T(8,128)(2,1)S(1)} %all-to-all-done.3.w0), channel_id=1, source_target_pairs={{0,4},{2,6},{4,0},{6,2},{1,5},{3,7},{5,1},{7,3},{8,12},{10,14},{12... | collective-permute-start | bytes 2359304 | tf_op jit(solution)/shard_map/ppermute | solution.py:474
  130.0 5.7 %collective-permute-start.13 = (bf16[16,128]{1,0:T(8,128)(2,1)}, bf16[16,128]{1,0:T(8,128)(2,1)S(1)}, u32[]{:S(2)}, u32[]{:S(2)}) collective-permute-start(bf16[16,128]{1,0:T(8,128)(2,1)} %get-tuple-element.51), channel_id=1, source_target_pairs={{0,32},{32,64},{64,96},{96,128},{128,160},{160,192},{192,224},{1,3... | collective-permute-start | bytes 12296 | tf_op jit(solution)/shard_map/ppermute | solution.py:546
  133.1 5.0 %collective-permute-start.14 = (bf16[16,128]{1,0:T(8,128)(2,1)}, bf16[16,128]{1,0:T(8,128)(2,1)S(1)}, u32[]{:S(2)}, u32[]{:S(2)}) collective-permute-start(bf16[16,128]{1,0:T(8,128)(2,1)} %get-tuple-element.52), channel_id=1, source_target_pairs={{32,0},{64,32},{96,64},{128,96},{160,128},{192,160},{224,192},{33,... | collective-permute-start | bytes 12296 | tf_op jit(solution)/shard_map/ppermute | solution.py:547
  135.8 2.3 %copy-start.24 = (bf16[16,128]{1,0:T(8,128)(2,1)}, bf16[16,128]{1,0:T(8,128)(2,1)S(1)}, u32[]{:S(2)}) copy-start(bf16[16,128]{1,0:T(8,128)(2,1)S(1)} %collective-permute-done.13.low) | copy-start | bytes 12292
  138.1 0.6 copy-start.25
  141.0 17.3 %copy-start.29 = (bf16[128,128]{1,0:T(8,128)(2,1)S(1)}, bf16[128,128]{1,0:T(8,128)(2,1)}, u32[]{:S(2)}) copy-start(bf16[128,128]{1,0:T(8,128)(2,1)} %get-tuple-element.55) | copy-start | bytes 98308
  141.0 19.2 %copy-start.28 = (bf16[128,128]{1,0:T(8,128)(2,1)S(1)}, bf16[128,128]{1,0:T(8,128)(2,1)}, u32[]{:S(2)}) copy-start(bf16[128,128]{1,0:T(8,128)(2,1)} %get-tuple-element.56) | copy-start | bytes 98308
  141.0 31.4 %copy-start.32 = (f32[256]{0:T(256)S(1)}, f32[256]{0:T(256)}, u32[]{:S(2)}) copy-start(f32[256]{0:T(256)} %param.34) | copy-start | bytes 3076
  141.0 19.2 %collective-permute-start.15 = (bf16[128,128]{1,0:T(8,128)(2,1)}, bf16[128,128]{1,0:T(8,128)(2,1)S(1)}, u32[]{:S(2)}, u32[]{:S(2)}) collective-permute-start(bf16[128,128]{1,0:T(8,128)(2,1)} %get-tuple-element.54), channel_id=1, source_target_pairs={{0,8},{8,16},{16,24},{24,0},{1,9},{9,17},{17,25},{25,1},{2,10},{10... | collective-permute-start | bytes 98312 | tf_op jit(solution)/shard_map/ppermute | solution.py:474
  142.2 0.8 copy-start.3
  152.0 30.8 %all-to-all-start.1 = ((bf16[8,64,128]{2,1,0:T(8,128)(2,1)}), bf16[8,64,128]{2,1,0:T(8,128)(2,1)S(1)}, u32[]{:S(2)}, u32[]{:S(2)}) async-start(bf16[8,64,128]{2,1,0:T(8,128)(2,1)} %get-tuple-element.38), calls=%async_computation.1 | async-start | bytes 262144 | tf_op jit(solution)/shard_map/all_to_all | solution.py:482
  158.3 3.8 %collective-permute-start.16 = (bf16[128,128]{1,0:T(8,128)(2,1)S(1)}, bf16[128,128]{1,0:T(8,128)(2,1)S(1)}, u32[]{:S(2)}, u32[]{:S(2)}) collective-permute-start(bf16[128,128]{1,0:T(8,128)(2,1)S(1)} %copy-done.29), channel_id=1, source_target_pairs={{0,24},{8,0},{16,8},{24,16},{1,25},{9,1},{17,9},{25,17},{2,26},{10... | collective-permute-start | bytes 98312 | tf_op jit(solution)/shard_map/ppermute | solution.py:474
  160.2 4.4 %copy-start.16 = (bf16[128,128]{1,0:T(8,128)(2,1)}, bf16[128,128]{1,0:T(8,128)(2,1)S(1)}, u32[]{:S(2)}) copy-start(bf16[128,128]{1,0:T(8,128)(2,1)S(1)} %collective-permute-done.15.c1) | copy-start | bytes 98308
  160.2 4.4 %collective-permute-start.17 = (bf16[128,128]{1,0:T(8,128)(2,1)S(1)}, bf16[128,128]{1,0:T(8,128)(2,1)S(1)}, u32[]{:S(2)}, u32[]{:S(2)}) collective-permute-start(bf16[128,128]{1,0:T(8,128)(2,1)S(1)} %copy-done.28), channel_id=1, source_target_pairs={{0,16},{8,24},{16,0},{24,8},{1,17},{9,25},{17,1},{25,9},{2,18},{10... | collective-permute-start | bytes 98312 | tf_op jit(solution)/shard_map/ppermute | solution.py:474
  162.1 2.4 %copy-start.17 = (bf16[128,128]{1,0:T(8,128)(2,1)}, bf16[128,128]{1,0:T(8,128)(2,1)S(1)}, u32[]{:S(2)}) copy-start(bf16[128,128]{1,0:T(8,128)(2,1)S(1)} %collective-permute-done.16.c2) | copy-start | bytes 98308
  164.5 0.6 copy-start.18
  166.8 22.4 %collective-permute-start.18 = (f32[128,128]{1,0:T(8,128)}, f32[128,128]{1,0:T(8,128)S(1)}, u32[]{:S(2)}, u32[]{:S(2)}) collective-permute-start(f32[128,128]{1,0:T(8,128)} %get-tuple-element.58.mine), channel_id=1, source_target_pairs={{0,1},{1,0},{2,3},{3,2},{4,5},{5,4},{6,7},{7,6},{8,9},{9,8},{10,11... | collective-permute-start | bytes 196616 | tf_op jit(solution)/shard_map/ppermute | solution.py:478
  182.8 0.7 copy-start.4
  186.4 7.3 %collective-permute-start.10 = (bf16[128,64]{1,0:T(8,128)(2,1)}, bf16[128,64]{1,0:T(8,128)(2,1)S(1)}, u32[]{:S(2)}, u32[]{:S(2)}) collective-permute-start(bf16[128,64]{1,0:T(8,128)(2,1)} %get-tuple-element.47), channel_id=1, source_target_pairs={{0,8},{8,16},{16,24},{24,0},{1,9},{9,17},{17,25},{25,1},{2,10},{10... | collective-permute-start | bytes 49160 | tf_op jit(solution)/shard_map/ppermute | solution.py:474
  186.5 7.3 %collective-permute-start.11 = (bf16[128,64]{1,0:T(8,128)(2,1)}, bf16[128,64]{1,0:T(8,128)(2,1)S(1)}, u32[]{:S(2)}, u32[]{:S(2)}) collective-permute-start(bf16[128,64]{1,0:T(8,128)(2,1)} %get-tuple-element.48), channel_id=1, source_target_pairs={{0,24},{8,0},{16,8},{24,16},{1,25},{9,1},{17,9},{25,17},{2,26},{10... | collective-permute-start | bytes 49160 | tf_op jit(solution)/shard_map/ppermute | solution.py:474
  189.1 4.6 %collective-permute-start.12 = (bf16[128,64]{1,0:T(8,128)(2,1)}, bf16[128,64]{1,0:T(8,128)(2,1)S(1)}, u32[]{:S(2)}, u32[]{:S(2)}) collective-permute-start(bf16[128,64]{1,0:T(8,128)(2,1)} %get-tuple-element.49), channel_id=1, source_target_pairs={{0,16},{8,24},{16,0},{24,8},{1,17},{9,25},{17,1},{25,9},{2,18},{10... | collective-permute-start | bytes 49160 | tf_op jit(solution)/shard_map/ppermute | solution.py:474
  189.1 0.6 copy-start.7
  193.7 0.6 copy-start.10
  193.7 0.6 copy-start.11
  193.8 0.6 copy-start.12
  198.1 2.9 %collective-permute-start.22 = (bf16[64,2048]{1,0:T(8,128)(2,1)}, bf16[64,2048]{1,0:T(8,128)(2,1)S(1)}, u32[]{:S(2)}, u32[]{:S(2)}) collective-permute-start(bf16[64,2048]{1,0:T(8,128)(2,1)} %get-tuple-element.60), channel_id=1, source_target_pairs={{0,1},{1,0},{2,3},{3,2},{4,5},{5,4},{6,7},{7,6},{8,9},{9,8},{10,11... | collective-permute-start | bytes 786440 | tf_op jit(solution)/shard_map/ppermute | solution.py:478
